TPU v7x, 32 devices: a whole 2x2x4 slice. The times are simulated.
32 devices in a mesh: ep: 8 (over z, x), tp: 4 (over y, core).
Axes of the slice: x: 2, y: 2, z: 4, core: 2. Of those that a mesh axis runs over, the one named last changes fastest.
Arguments:
- hidden: bfloat16 [32, 2048], P('ep'), may hold values from -6 to 6
- attn_gain: float32 [2048], replicated, may hold values from 0.3 to 3
- query_weight: bfloat16 [2048, 2048], P('ep', 'tp'), may hold values from -0.125 to 0.125
- head_bias: float32 [16], replicated, may hold values from -10 to -4
- key_cache: bfloat16 [32, 4, 1024, 128], P('ep', 'tp'), may hold values from -6 to 6
- value_cache: bfloat16 [32, 4, 1024, 128], P('ep', 'tp'), may hold values from -7 to 7
- lengths: int32 [32], P('ep'), may hold values from 256 to 1024, as said below
- out_weight: bfloat16 [2048, 2048], P('tp', 'ep'), may hold values from -0.125 to 0.125
- moe_gain: float32 [2048], replicated, may hold values from 0.1 to 1.9
- route_group: int32 [32], P('ep'), may hold values from 0 to 1, as said below
- route_inner: int32 [32, 2], P('ep'), may hold values from 0 to 3, as said below
- route_weight: bfloat16 [32, 2], P('ep'), may hold values from 0.25 to 1
- gate_w: bfloat16 [8, 2048, 768], P('ep', None, 'tp'), may hold values from -0.125 to 0.125
- up_w: bfloat16 [8, 2048, 768], P('ep', None, 'tp'), may hold values from -0.125 to 0.125
- down_w: bfloat16 [8, 768, 2048], P('ep', 'tp'), may hold values from -0.21875 to 0.21875
Outputs:
- mixed: bfloat16 [32, 2048], P('ep', 'tp')
Inputs may be any that keep to these rules, and one draw needn't show every extreme that they name: `lengths`: some sequence has length 1024 in every draw. Within the rows of one device (aligned blocks of 4 rows) no expert route_group * 4 + route_inner is named twice; one expert is named in every block. `route_inner`: the 2 entries of a row differ.
All inputs are finite; a program needn't handle non-finite values.
Results may differ from a plain program's by a relative error of at most 0.013.
Values may be sent and summed in bfloat16 or wider, within the bound.
No kernel may reach another device: no remote copies, remote signals or barrier semaphores. Data moves between devices by JAX's collectives and lax.ppermute only.
A program may use at most 64 MiB of HBM per device.

v0:
```python
import jax
import jax.numpy as jnp
from jax import lax
from jax.sharding import PartitionSpec as P

rms_epsilon = 1e-06


def rms_scale(values, gain):
    wide = values.astype(jnp.float32)
    scaled = wide * lax.rsqrt(jnp.mean(wide * wide, axis=-1, keepdims=True) + rms_epsilon)
    return (scaled * gain).astype(jnp.bfloat16)


def body(
    hidden,
    attn_gain,
    query_weight,
    head_bias,
    key_cache,
    value_cache,
    lengths,
    out_weight,
    moe_gain,
    route_group,
    route_inner,
    route_weight,
    gate_w,
    up_w,
    down_w,
):
    n_tp = lax.axis_size("tp")
    n_ep = lax.axis_size("ep")
    tokens = hidden.shape[0]
    d_model = hidden.shape[1]
    normed = rms_scale(hidden, attn_gain)
    feature_block = lax.all_to_all(normed, "ep", split_axis=1, concat_axis=0, tiled=True)
    queries = lax.psum_scatter(
        jnp.dot(feature_block, query_weight, preferred_element_type=jnp.float32),
        "ep",
        scatter_dimension=0,
        tiled=True,
    ).astype(jnp.bfloat16)
    head_size = key_cache.shape[3]
    local_kv = key_cache.shape[1]
    cache_len = key_cache.shape[2]
    local_heads = queries.shape[1] // head_size
    group_heads = local_heads // local_kv
    queries = queries.reshape(tokens, local_kv, group_heads, head_size)
    own_bias = lax.dynamic_slice_in_dim(
        head_bias, lax.axis_index("tp") * local_heads, local_heads, 0
    )
    own_bias = own_bias.reshape(local_kv, group_heads)
    scores = jnp.einsum(
        "tkgd,tkpd->tkgp", queries, key_cache, preferred_element_type=jnp.float32
    ) * head_size ** (-0.5)
    scores = scores + own_bias[None, :, :, None]
    position = jnp.arange(cache_len, dtype=jnp.int32)
    visible = position[None, None, None, :] < lengths[:, None, None, None]
    log_keep = jnp.where(visible, jax.nn.log_sigmoid(-scores), 0.0)
    later_sum = lax.cumsum(log_keep, axis=3, reverse=True) - log_keep
    weight = jnp.where(visible, jnp.exp(jax.nn.log_sigmoid(scores) + later_sum), 0.0).astype(
        jnp.bfloat16
    )
    heads_out = jnp.einsum(
        "tkgp,tkpd->tkgd", weight, value_cache, preferred_element_type=jnp.float32
    )
    heads_out = heads_out.astype(jnp.bfloat16).reshape(tokens, -1)
    partial_value = jnp.dot(
        heads_out,
        lax.all_gather(out_weight, "ep", axis=1, tiled=True),
        preferred_element_type=jnp.float32,
    )
    rounded = lax.optimization_barrier(partial_value.astype(jnp.bfloat16)).astype(jnp.float32)
    attended = lax.psum(rounded.astype(jnp.bfloat16), "tp").astype(jnp.float32)
    residual = (hidden.astype(jnp.float32) + attended).astype(jnp.bfloat16)
    normed_two = rms_scale(residual, moe_gain)
    per_device = gate_w.shape[0]
    experts = per_device * n_ep
    group_count = max(2, experts // 32)
    group_size = experts // group_count
    chosen = route_group[:, None] * group_size + route_inner
    matches = chosen[:, :, None] == jnp.arange(experts, dtype=jnp.int32)[None, None, :]
    picked = jnp.any(matches, axis=1).astype(jnp.bfloat16)
    mixing = jnp.sum(
        jnp.where(matches, route_weight[:, :, None].astype(jnp.float32), 0.0), axis=1
    ).astype(jnp.bfloat16)
    part_width = d_model // n_tp
    outgoing = jnp.einsum("te,td->ed", picked, normed_two, preferred_element_type=jnp.float32)
    outgoing = outgoing.astype(jnp.bfloat16).reshape(n_ep, per_device, d_model)
    arrived = lax.all_to_all(outgoing, "ep", split_axis=0, concat_axis=0, tiled=True)
    gated_in = jnp.einsum("sed,edf->sef", arrived, gate_w, preferred_element_type=jnp.float32)
    up_proj = jnp.einsum("sed,edf->sef", arrived, up_w, preferred_element_type=jnp.float32)
    activated = (jax.nn.silu(gated_in) * up_proj).astype(jnp.bfloat16)
    down_out = jnp.einsum("sef,efd->sed", activated, down_w, preferred_element_type=jnp.float32)
    down_rounded = lax.optimization_barrier(down_out.astype(jnp.bfloat16)).astype(jnp.float32)
    summed = lax.psum_scatter(
        down_rounded.astype(jnp.bfloat16), "tp", scatter_dimension=2, tiled=True
    )
    returned = lax.all_to_all(summed, "ep", split_axis=0, concat_axis=0, tiled=True).reshape(
        experts, part_width
    )
    routed = jnp.dot(mixing, returned, preferred_element_type=jnp.float32)
    own_residual = lax.dynamic_slice_in_dim(
        residual, lax.axis_index("tp") * part_width, part_width, 1
    )
    return (own_residual.astype(jnp.float32) + routed).astype(jnp.bfloat16)


def solution(mesh):
    placed = (
        P("ep", None),
        P(),
        P("ep", "tp"),
        P(),
        P("ep", "tp", None, None),
        P("ep", "tp", None, None),
        P("ep"),
        P("tp", "ep"),
        P(),
        P("ep"),
        P("ep", None),
        P("ep", None),
        P("ep", None, "tp"),
        P("ep", None, "tp"),
        P("ep", "tp", None),
    )
    return jax.shard_map(body, mesh=mesh, in_specs=placed, out_specs=P("ep", "tp"), check_vma=False)
```

profile of v0, /device:TPU:0, one launch (start us, length us, event | category | flops | bytes accessed | tf_op | source)
XLA Modules:
  0.0 150.5 jit_solution(8893848438040312585)
XLA Ops:
  6.5 0.0 copy-start
  6.5 0.0 all-gather.2.cloned.1.call-start
  6.5 0.7 all-gather.2.cloned.1.call-update
  7.3 0.8 fusion.25
  8.1 1.4 fusion.27
  9.5 7.3 %all-to-all-start = ((bf16[4,8,256]{2,0,1:T(4,128)(2,1)}), bf16[4,8,256]{2,0,1:T(4,128)(2,1)S(1)}, u32[]{:S(2)}, u32[]{:S(2)}) async-start(bf16[4,8,256]{2,0,1:T(4,128)(2,1)} %bitcast), calls=%async_computation | async-start | bytes 32768 | tf_op jit(solution)/shard_map/all_to_all | solution.py:37
  16.8 0.0 reduce-scatter.2.cloned.1.call-start
  16.8 0.7 broadcast_multiply_fusion
  17.5 0.7 broadcast_add_fusion
  18.2 0.0 copy-start.6
  18.2 0.7 iota_compare_fusion
  18.9 0.0 copy-start.5
  18.9 0.6 fusion.51
  19.5 0.7 dynamic_slice.6
  20.2 1.3 dynamic-slice
  22.1 1.4 all-to-all-done
  23.5 0.0 copy-done.6
  23.5 1.1 fusion.57
  24.6 37.7 %all-reduce = bf16[32,512]{1,0:T(8,128)(2,1)S(1)} all-reduce(f32[32,512]{1,0:T(8,128)S(1)} %fusion.57), channel_id=2, replica_groups=mesh['ep'=8,'tp'=4] {'ep'}, use_global_device_ids=true, to_apply=%region_1.0.clone | all-reduce | flops 16384 | bytes 98304
  62.3 0.0 copy-done
  62.3 0.4 fusion.21
  62.7 0.0 copy-done.5
  62.8 0.0 copy-start.4
  62.8 19.8 %reduce-window.6 = f32[4,1,4,8,128]{4,3,2,1,0:T(8,128)S(1)} reduce-window(f32[4,1,4,8,128]{4,3,2,1,0:T(8,128)S(1)} %bitcast.82, f32[]{:T(128)} %constant.12.clone.1), window={size=1x1x1x1x128 pad=0_0x0_0x0_0x0_0x0_127}, to_apply=%region_2.3 | reduce-window | flops 2080768 | bytes 131076 | tf_op jit(solution)/shard_map/reduce-window
  82.6 0.1 slice_reduce_fusion
  82.7 0.7 reduce-window.9
  83.4 0.1 slice_bitcast_fusion
  83.5 0.0 copy-start.1
  83.5 0.1 broadcast.72
  83.6 0.7 reshape.151
  84.3 0.0 copy-start.2
  84.3 0.0 copy-start.3
  84.3 2.4 %fusion.6 = bf16[1,4,4,128]{3,2,1,0:T(4,128)(2,1)} fusion(bf16[4,1,1024,128]{3,2,1,0:T(8,128)(2,1)} %param.20, f32[4,4,1024]{2,1,0:T(4,128)S(1)} %reshape.148, f32[4,4,1024]{2,1,0:T(4,128)} %reshape.151, f32[4,4,1024]{2,1,0:T(4,128)S(1)} %get-tuple-element.8, pred[4,1024]{1,0:T(4,128)(4,1)} %copy-done.5), kind=kOutput, calls=%fused_computation.14 | convolution fusion | flops 4540416 | bytes 1253376 | tf_op jit(solution)/shard_map/tkgp,tkpd->tkgd/dot_general | solution.py:65
  86.6 0.0 copy-start.8
  86.6 0.0 copy-start.7
  86.6 0.0 all-gather.2.cloned.1.call-done
  86.6 2.0 %convolution_convert_fusion.2 = bf16[4,2048]{1,0:T(4,128)(2,1)S(1)} fusion(bf16[512,2048]{1,0:T(8,128)(2,1)} %all-gather.2.cloned.1.call-done, bf16[1,4,4,128]{3,2,1,0:T(4,128)(2,1)} %fusion.6), kind=kOutput, calls=%fused_computation.4 | convolution fusion | flops 8396800 | bytes 2117632 | tf_op jit(solution)/shard_map/dot_general | solution.py:69
  88.6 10.1 %psum.7 = bf16[4,2048]{1,0:T(4,128)(2,1)S(1)} all-reduce(bf16[4,2048]{1,0:T(4,128)(2,1)S(1)} %convolution_convert_fusion.2), channel_id=1, replica_groups=mesh['ep'=8,'tp'=4] {'tp'}, use_global_device_ids=true, to_apply=%region_4.5 | all-reduce | flops 8192 | bytes 32768 | tf_op jit(solution)/shard_map/psum | solution.py:75
  98.7 0.0 copy-done.4
  98.7 0.1 fusion.22
  98.9 0.9 fusion
  99.8 0.5 broadcast.80
  100.3 0.7 reduce.2
  101.0 9.1 %all_to_all.29 = bf16[8,2,1024]{2,1,0:T(2,128)(2,1)S(1)} all-to-all(bf16[8,2,1024]{2,1,0:T(2,128)(2,1)S(1)} %reshape.163), channel_id=1, replica_groups=mesh['ep'=8,'tp'=4] {'ep'}, dimensions={0} | all-to-all | bytes 65536 | tf_op jit(solution)/shard_map/all_to_all | solution.py:91
  110.1 0.0 copy-done.1
  110.1 0.3 convolution_bitcast_fusion.1
  110.4 0.0 copy-done.2
  110.4 0.0 copy-done.3
  110.4 1.3 fusion.1
  111.7 0.0 reduce-scatter.2.cloned.1.call-update
  111.7 0.0 copy-done.8
  111.8 17.1 %reduce-scatter.2.cloned.1.call-done = bf16[8,1,512]{2,0,1:T(8,128)(2,1)} async-done(((bf16[8,1,2048]{2,0,1:T(8,128)(2,1)}), bf16[8,1,512]{2,0,1:T(8,128)(2,1)}) %reduce-scatter.2.cloned.1.call-update) | async-done | bytes 8208 | tf_op jit(solution)/shard_map/reduce_scatter | solution.py:97
  128.9 1.3 reduce.3
  130.2 0.6 reshape.165
  130.9 5.5 %all-to-all-start.2 = ((bf16[8,2,256]{2,1,0:T(2,128)(2,1)}), bf16[8,2,256]{2,1,0:T(2,128)(2,1)S(1)}, u32[]{:S(2)}, u32[]{:S(2)}) async-start(bf16[8,2,256]{2,1,0:T(2,128)(2,1)} %reshape.165), calls=%async_computation.3 | async-start | bytes 16384 | tf_op jit(solution)/shard_map/all_to_all | solution.py:100
  136.4 0.0 copy-done.7
  136.4 0.1 select_reduce_fusion
  136.5 6.4 %all-to-all-done.2 = bf16[8,2,256]{2,1,0:T(2,128)(2,1)S(1)} async-done(((bf16[8,2,256]{2,1,0:T(2,128)(2,1)}), bf16[8,2,256]{2,1,0:T(2,128)(2,1)S(1)}, u32[]{:S(2)}, u32[]{:S(2)}) %all-to-all-start.2) | async-done | bytes 8224 | tf_op jit(solution)/shard_map/all_to_all | solution.py:100
  142.9 0.7 fusion.4
  (11 shorter events, 0.2 us)
Async XLA Ops:
  6.5 55.8 %copy-start = (bf16[4,1,1024,128]{3,2,1,0:T(8,128)(2,1)S(1)}, bf16[4,1,1024,128]{3,2,1,0:T(8,128)(2,1)}, u32[]{:S(2)}) copy-start(bf16[4,1,1024,128]{3,2,1,0:T(8,128)(2,1)} %param.19) | copy-start | bytes 3145732
  6.5 80.1 %all-gather.2.cloned.1.call-start = ((), (), s32[]{:S(2)}) async-start(), calls=%async_computation.4 | async-start | bytes 2359296 | tf_op jit(solution)/shard_map/all_gather | solution.py:71
  9.5 14.0 %all-to-all-start = ((bf16[4,8,256]{2,0,1:T(4,128)(2,1)}), bf16[4,8,256]{2,0,1:T(4,128)(2,1)S(1)}, u32[]{:S(2)}, u32[]{:S(2)}) async-start(bf16[4,8,256]{2,0,1:T(4,128)(2,1)} %bitcast), calls=%async_computation | async-start | bytes 32768 | tf_op jit(solution)/shard_map/all_to_all | solution.py:37
  16.8 112.1 %reduce-scatter.2.cloned.1.call-start = ((), (), s32[]{:S(2)}) async-start(), calls=%async_computation.5 | async-start | bytes 40960 | tf_op jit(solution)/shard_map/reduce_scatter | solution.py:97
  18.2 5.3 %copy-start.6 = (s32[4,2]{0,1:T(2,128)}, s32[4,2]{0,1:T(2,128)S(1)}, u32[]{:S(2)}) copy-start(s32[4,2]{0,1:T(2,128)S(1)} %broadcast_add_fusion) | copy-start | bytes 100
  18.9 43.8 %copy-start.5 = (pred[4,1024]{1,0:T(4,128)(4,1)}, pred[4,1024]{1,0:T(4,128)(4,1)S(1)}, u32[]{:S(2)}) copy-start(pred[4,1024]{1,0:T(4,128)(4,1)S(1)} %iota_compare_fusion) | copy-start | bytes 12292
  62.8 36.0 %copy-start.4 = (bf16[4,2048]{1,0:T(4,128)(2,1)S(1)}, bf16[4,2048]{1,0:T(4,128)(2,1)}, u32[]{:S(2)}) copy-start(bf16[4,2048]{1,0:T(4,128)(2,1)} %param.15) | copy-start | bytes 49156
  83.5 26.6 %copy-start.1 = (bf16[1,2048,192]{1,2,0:T(8,128)(2,1)S(1)}, bf16[1,2048,192]{1,2,0:T(8,128)(2,1)}, u32[]{:S(2)}) copy-start(bf16[1,2048,192]{1,2,0:T(8,128)(2,1)} %param.27) | copy-start | bytes 2359300
  84.3 26.2 %copy-start.2 = (bf16[1,192,2048]{2,1,0:T(8,128)(2,1)S(1)}, bf16[1,192,2048]{2,1,0:T(8,128)(2,1)}, u32[]{:S(2)}) copy-start(bf16[1,192,2048]{2,1,0:T(8,128)(2,1)} %param.29) | copy-start | bytes 2359300
  84.3 26.2 %copy-start.3 = (bf16[1,2048,192]{1,2,0:T(8,128)(2,1)S(1)}, bf16[1,2048,192]{1,2,0:T(8,128)(2,1)}, u32[]{:S(2)}) copy-start(bf16[1,2048,192]{1,2,0:T(8,128)(2,1)} %param.28) | copy-start | bytes 2359300
  86.6 25.1 %copy-start.8 = (bf16[4,2]{0,1:T(2,128)(2,1)S(1)}, bf16[4,2]{0,1:T(2,128)(2,1)}, u32[]{:S(2)}) copy-start(bf16[4,2]{0,1:T(2,128)(2,1)} %param.26) | copy-start | bytes 52
  86.6 49.8 %copy-start.7 = (s32[4,2]{0,1:T(2,128)S(1)}, s32[4,2]{0,1:T(2,128)}, u32[]{:S(2)}) copy-start(s32[4,2]{0,1:T(2,128)} %copy-done.6) | copy-start | bytes 100
  130.9 12.0 %all-to-all-start.2 = ((bf16[8,2,256]{2,1,0:T(2,128)(2,1)}), bf16[8,2,256]{2,1,0:T(2,128)(2,1)S(1)}, u32[]{:S(2)}, u32[]{:S(2)}) async-start(bf16[8,2,256]{2,1,0:T(2,128)(2,1)} %reshape.165), calls=%async_computation.3 | async-start | bytes 16384 | tf_op jit(solution)/shard_map/all_to_all | solution.py:100
Sparse Core Ops, SparseCore 0:
  9.4 54.2 all-gather.1
  111.9 16.9 reduce-scatter.1
where the time goes:
time: 151 us; the launch traced here: 150 us
  blocking collectives  56.9 us (38%)
  other arithmetic  27.7 us (18%)
  waiting for transfers between devices  25.6 us (17%)
  between operations  14.1 us (9%)
  starting transfers between devices  12.8 us (8%)
  matrix products  9.09 us (6%)
  local copies, waits for them, and re-layouts  4.21 us (3%)
    unnamed x1, blocking collectives  37.7 us
    another operation x2, other arithmetic  20.5 us
    reduce_scatter x1, waiting for transfers between devices, body(): lax.psum_scatter(down_rounded.astype(jnp.bfloat16), 'tp', scatter_dimensi...  17.1 us
    psum x1, blocking collectives, body(): attended = lax.psum(rounded.astype(jnp.bfloat16), 'tp').astype(jnp.float32)  10.1 us
    all_to_all x1, blocking collectives, body(): lax.all_to_all(outgoing, 'ep', split_axis=0, concat_axis=0, tiled=True)  9.06 us
    all_to_all x1, starting transfers between devices, body(): lax.all_to_all(normed, 'ep', split_axis=1, concat_axis=0, tiled=True)  7.28 us
    all_to_all x1, waiting for transfers between devices, body(): lax.all_to_all(summed, 'ep', split_axis=0, concat_axis=0, tiled=True)  6.43 us
    all_to_all x1, starting transfers between devices, body(): lax.all_to_all(summed, 'ep', split_axis=0, concat_axis=0, tiled=True)  5.51 us
  transfers between devices with their start and end apart: 4, of which 3 were waited for; matrix products, arithmetic and copies ran while one was open for 22% of the time, Pallas kernels for 0%

commit v1 on v0

v1 whole, which is shorter than its diff:
```python
import jax
import jax.numpy as jnp
from jax import lax
from jax.sharding import PartitionSpec as P

rms_epsilon = 1e-06


def body(
    hidden,
    attn_gain,
    query_weight,
    head_bias,
    key_cache,
    value_cache,
    lengths,
    out_weight,
    moe_gain,
    route_group,
    route_inner,
    route_weight,
    gate_w,
    up_w,
    down_w,
):
    f32, bf16 = jnp.float32, jnp.bfloat16
    n_tp = lax.axis_size("tp")
    n_ep = lax.axis_size("ep")
    tokens, d_model = hidden.shape
    rows = query_weight.shape[0]
    per_device = gate_w.shape[0]
    experts = per_device * n_ep
    group_count = max(2, experts // 32)
    group_size = experts // group_count
    top_k = route_inner.shape[1]
    chosen = route_group[:, None] * group_size + route_inner

    blocks = hidden.reshape(tokens, n_ep, rows).transpose(1, 0, 2).reshape(n_ep, tokens * rows)
    ids = jnp.broadcast_to(chosen.astype(bf16).reshape(1, tokens * top_k), (n_ep, tokens * top_k))
    ids = jnp.pad(ids, ((0, 0), (0, 128 - tokens * top_k)))
    packed = jnp.concatenate([blocks, ids], axis=1)
    packed = lax.all_to_all(packed, "ep", split_axis=0, concat_axis=0, tiled=True)
    all_tokens = n_ep * tokens
    features = packed[:, : tokens * rows].reshape(all_tokens, rows)
    all_chosen = packed[:, tokens * rows : tokens * (rows + top_k)].reshape(all_tokens, top_k)
    all_chosen = all_chosen.astype(jnp.int32)

    ep_index = lax.axis_index("ep")
    gain_block = lax.dynamic_slice_in_dim(attn_gain, ep_index * rows, rows, 0)
    scaled = (features.astype(f32) * gain_block).astype(bf16)
    parts = jnp.dot(scaled, query_weight, preferred_element_type=f32)
    width = parts.shape[1]

    parts = lax.all_to_all(
        parts.reshape(n_ep, tokens * width), "ep", split_axis=0, concat_axis=0, tiled=True
    )
    wide = hidden.astype(f32)
    row_scale = lax.rsqrt(jnp.mean(wide * wide, axis=-1, keepdims=True) + rms_epsilon)
    queries = parts.sum(axis=0).reshape(tokens, width) * row_scale
    queries = queries.astype(bf16)

    head_size = key_cache.shape[3]
    local_kv = key_cache.shape[1]
    cache_len = key_cache.shape[2]
    local_heads = width // head_size
    group_heads = local_heads // local_kv
    queries = queries.reshape(tokens, local_kv, group_heads, head_size)
    own_bias = lax.dynamic_slice_in_dim(
        head_bias, lax.axis_index("tp") * local_heads, local_heads, 0
    )
    own_bias = own_bias.reshape(local_kv, group_heads)
    scores = jnp.einsum(
        "tkgd,tkpd->tkgp", queries, key_cache, preferred_element_type=f32
    ) * head_size ** (-0.5)
    scores = scores + own_bias[None, :, :, None]
    position = jnp.arange(cache_len, dtype=jnp.int32)
    visible = position[None, None, None, :] < lengths[:, None, None, None]
    soft = jnp.log1p(jnp.exp(-jnp.abs(scores)))
    log_keep = jnp.where(visible, -jnp.maximum(scores, 0.0) - soft, 0.0)
    n_chunk = cache_len // 128
    chunked = log_keep.reshape(tokens, local_kv, group_heads, n_chunk, 128)
    lower = (jnp.arange(128)[:, None] > jnp.arange(128)[None, :]).astype(f32)
    inner = jnp.einsum("tkgcp,pq->tkgcq", chunked, lower, precision=lax.Precision.HIGHEST)
    totals = chunked.sum(axis=-1)
    later_chunks = jnp.arange(n_chunk)[:, None] > jnp.arange(n_chunk)[None, :]
    outer = jnp.where(later_chunks, totals[..., :, None], 0.0).sum(axis=-2)
    later_sum = (inner + outer[..., None]).reshape(scores.shape)
    weight = jnp.where(visible, jnp.exp(jnp.minimum(scores, 0.0) - soft + later_sum), 0.0)
    heads_out = jnp.einsum(
        "tkgp,tkpd->tkgd", weight.astype(bf16), value_cache, preferred_element_type=f32
    )
    heads_out = heads_out.astype(bf16).reshape(1, tokens * width)

    gathered = lax.all_to_all(
        jnp.broadcast_to(heads_out, (n_ep, tokens * width)), "ep", split_axis=0, concat_axis=0, tiled=True
    ).reshape(all_tokens, width)
    partial = jnp.dot(gathered, out_weight, preferred_element_type=f32)
    columns = out_weight.shape[1]
    partial = (partial + features.astype(f32) * (1.0 / n_tp)).astype(bf16)

    by_block = all_chosen.reshape(n_ep, tokens, top_k)
    hits = by_block[None] == jnp.arange(experts, dtype=jnp.int32)[:, None, None, None]
    hits = jnp.any(hits, axis=3).astype(bf16)
    routed = jnp.einsum(
        "ebt,btc->ebc", hits, partial.reshape(n_ep, tokens, columns), preferred_element_type=f32
    ).astype(bf16)
    routed = routed.reshape(n_ep, per_device * n_ep * columns)
    message = jnp.concatenate([routed, partial.reshape(n_ep, tokens * columns)], axis=1)
    length = message.shape[1]
    message = jnp.broadcast_to(message[:, None], (n_ep, n_tp, length)).reshape(n_ep * n_tp, length)
    received = lax.all_to_all(message, ("ep", "tp"), split_axis=0, concat_axis=0, tiled=True)
    received = received.reshape(n_ep, n_tp, per_device * n_ep + tokens, columns)
    summed = received.astype(f32).sum(axis=1)
    residual = summed.transpose(1, 0, 2).reshape(per_device * n_ep + tokens, d_model)
    arrived = residual[: per_device * n_ep]
    arrived = arrived * lax.rsqrt(jnp.mean(arrived * arrived, axis=-1, keepdims=True) + rms_epsilon)
    arrived = (arrived * moe_gain).astype(bf16).reshape(per_device, n_ep, d_model)
    gated_in = jnp.einsum("esd,edf->esf", arrived, gate_w, preferred_element_type=f32)
    up_proj = jnp.einsum("esd,edf->esf", arrived, up_w, preferred_element_type=f32)
    activated = (jax.nn.silu(gated_in) * up_proj).astype(bf16)
    down_out = jnp.einsum("esf,efd->sed", activated, down_w, preferred_element_type=f32).astype(bf16)

    part_width = d_model // n_tp
    down_out = down_out.reshape(n_ep, per_device, n_tp, part_width).transpose(0, 2, 1, 3)
    returned = lax.all_to_all(
        down_out.reshape(n_ep * n_tp, per_device * part_width), ("ep", "tp"), split_axis=0, concat_axis=0, tiled=True
    )
    returned = returned.reshape(n_ep, n_tp, per_device, part_width).astype(f32).sum(axis=1)
    returned = returned.reshape(experts, part_width)
    matches = chosen[:, :, None] == jnp.arange(experts, dtype=jnp.int32)[None, None, :]
    mixing = jnp.sum(jnp.where(matches, route_weight[:, :, None].astype(f32), 0.0), axis=1)
    mixed = jnp.sum(mixing[:, :, None] * returned[None], axis=1)
    own_residual = lax.dynamic_slice_in_dim(
        residual[per_device * n_ep :], lax.axis_index("tp") * part_width, part_width, 1
    )
    return (own_residual + mixed).astype(bf16)


def solution(mesh):
    placed = (
        P("ep", None),
        P(),
        P("ep", "tp"),
        P(),
        P("ep", "tp", None, None),
        P("ep", "tp", None, None),
        P("ep"),
        P("tp", "ep"),
        P(),
        P("ep"),
        P("ep", None),
        P("ep", None),
        P("ep", None, "tp"),
        P("ep", None, "tp"),
        P("ep", "tp", None),
    )
    return jax.shard_map(body, mesh=mesh, in_specs=placed, out_specs=P("ep", "tp"), check_vma=False)
```

time: 151 us -> 74.7 us (0.49)
  blocking collectives: 56.9 us -> 0 us
  other arithmetic: 27.7 us -> 11 us
  between operations: 14.1 us -> 0.4 us
  starting transfers between devices: 12.8 us -> 19.4 us
  waiting for transfers between devices: 25.6 us -> 31.7 us
  matrix products: 9.09 us -> 3.17 us
  local copies, waits for them, and re-layouts: 4.21 us -> 8.38 us
    unnamed x1 -> x0, blocking collectives: 37.7 us -> none
    all_to_all x2 -> x5, waiting for transfers between devices: 7.79 us -> 31.7 us  [the longest x1 7.7 us: body(): lax.all_to_all(message, ('ep', 'tp'), split_axis=0, concat_axis=0, tiled=...]
    another operation x2 -> x0, other arithmetic: 20.5 us -> none
    reduce_scatter x1 -> x0, waiting for transfers between devices: 17.1 us -> none  [body(): lax.psum_scatter(down_rounded.astype(jnp.bfloat16), 'tp', scatter_dimensi...]
    psum x1 -> x0, blocking collectives: 10.1 us -> none  [body(): attended = lax.psum(rounded.astype(jnp.bfloat16), 'tp').astype(jnp.float32)]
    all_to_all x1 -> x0, blocking collectives: 9.06 us -> none  [body(): lax.all_to_all(outgoing, 'ep', split_axis=0, concat_axis=0, tiled=True)]
    all_to_all x2 -> x5, starting transfers between devices: 12.8 us -> 19.4 us  [the longest x1 7.28 us: body(): lax.all_to_all(packed, 'ep', split_axis=0, concat_axis=0, tiled=True)]
    dot_general x7, matrix products: 8.69 us -> 2.73 us  [the longest x1 1.45 us: body(): jnp.einsum('esf,efd->sed', activated, down_w, preferred_element_type=f32)]
  transfers between devices with their start and end apart: 4 -> 5, of which waited for: 3 -> 5; matrix products, arithmetic and copies ran while one was open for 22% -> 4% of each run, Pallas kernels for 0% -> 0%
where the time goes in v1:
time: 74.7 us; the launch traced here: 74 us
  waiting for transfers between devices  31.7 us (42%)
  starting transfers between devices  19.4 us (26%)
  other arithmetic  11 us (15%)
  local copies, waits for them, and re-layouts  8.38 us (11%)
  matrix products  3.17 us (4%)
    all_to_all x1, waiting for transfers between devices, body(): lax.all_to_all(message, ('ep', 'tp'), split_axis=0, concat_axis=0, tiled=...  7.7 us
    all_to_all x1, starting transfers between devices, body(): lax.all_to_all(packed, 'ep', split_axis=0, concat_axis=0, tiled=True)  7.28 us
    all_to_all x1, waiting for transfers between devices, body(): lax.all_to_all(parts.reshape(n_ep, tokens * width), 'ep', split_axis=0, c...  6.76 us
    all_to_all x1, waiting for transfers between devices, body(): lax.all_to_all(jnp.broadcast_to(heads_out, (n_ep, tokens * width)), 'ep',...  6.51 us
    all_to_all x1, waiting for transfers between devices, body(): lax.all_to_all(down_out.reshape(n_ep * n_tp, per_device * part_width), ('...  6.49 us
    unnamed x34, local copies, waits for them, and re-layouts  4.71 us
    all_to_all x1, waiting for transfers between devices, body(): lax.all_to_all(packed, 'ep', split_axis=0, concat_axis=0, tiled=True)  4.22 us
    all_to_all x1, starting transfers between devices, body(): lax.all_to_all(parts.reshape(n_ep, tokens * width), 'ep', split_axis=0, c...  3.35 us
  transfers between devices with their start and end apart: 5, of which 5 were waited for; matrix products, arithmetic and copies ran while one was open for 4% of the time, Pallas kernels for 0%

profile of v1, /device:TPU:0, one launch (start us, length us, event | category | flops | bytes accessed | tf_op | source)
XLA Modules:
  0.0 74.0 jit_solution(5059785536104352168)
XLA Ops:
  0.0 0.8 %broadcast_multiply_fusion = s32[4]{0:T(128)S(1)} fusion(s32[4]{0:T(128)} %param.24), kind=kLoop, calls=%fused_computation.64 | loop fusion | flops 4 | bytes 32 | tf_op jit(solution)/shard_map/mul | solution.py:36
  0.8 1.2 %fusion.32 = (bf16[4,2]{0,1:T(2,128)(2,1)S(1)}, s32[4,2]{0,1:T(2,128)}) fusion(s32[4,2]{0,1:T(2,128)} %param.25, s32[4]{0:T(128)S(1)} %broadcast_multiply_fusion), kind=kLoop, calls=%fused_computation.67 | loop fusion | flops 16 | bytes 96 | tf_op jit(solution)/shard_map/convert_element_type | solution.py:39
  2.0 0.1 copy.61
  2.1 0.1 broadcast_in_dim.47
  2.2 0.5 broadcast.188
  2.8 0.6 reduce.12
  3.4 0.7 reshape.340
  4.1 7.3 %all-to-all-start = ((bf16[8,2,576]{2,1,0:T(2,128)(2,1)}), bf16[8,2,576]{2,1,0:T(2,128)(2,1)S(1)}, u32[]{:S(2)}, u32[]{:S(2)}) async-start(bf16[8,2,576]{2,1,0:T(2,128)(2,1)} %reshape.340), calls=%async_computation | async-start | bytes 40960 | tf_op jit(solution)/shard_map/all_to_all | solution.py:42
  11.4 0.1 multiply_reduce_fusion.2
  11.5 0.7 iota_compare_fusion.2
  12.3 0.8 %dynamic_slice.9 = f32[256]{0:T(256)S(1)} dynamic-slice(f32[2048]{0:T(1024)} %param.16, s32[]{:T(128)S(6)} %select_n.34), dynamic_slice_sizes={256} | dynamic-slice | bytes 2052 | tf_op jit(solution)/shard_map/dynamic_slice | solution.py:49
  13.1 0.7 dynamic_slice.10
  13.8 4.2 %all-to-all-done = bf16[8,2,576]{2,1,0:T(2,128)(2,1)S(1)} async-done(((bf16[8,2,576]{2,1,0:T(2,128)(2,1)}), bf16[8,2,576]{2,1,0:T(2,128)(2,1)S(1)}, u32[]{:S(2)}, u32[]{:S(2)}) %all-to-all-start) | async-done | bytes 18464 | tf_op jit(solution)/shard_map/all_to_all | solution.py:42
  18.0 0.1 reshape.341
  18.2 0.1 fusion.20
  18.3 0.7 all_to_all.40
  19.0 3.3 %all-to-all-start.1 = ((f32[8,1,2048]{2,1,0:T(1,128)}), f32[8,1,2048]{2,1,0:T(1,128)S(1)}, u32[]{:S(2)}, u32[]{:S(2)}) async-start(f32[8,1,2048]{2,1,0:T(1,128)} %all_to_all.40), calls=%async_computation.1 | async-start | bytes 131072 | tf_op jit(solution)/shard_map/all_to_all | solution.py:54
  22.4 0.1 copy.64
  22.5 6.8 %all-to-all-done.1 = f32[8,1,2048]{2,1,0:T(1,128)S(1)} async-done(((f32[8,1,2048]{2,1,0:T(1,128)}), f32[8,1,2048]{2,1,0:T(1,128)S(1)}, u32[]{:S(2)}, u32[]{:S(2)}) %all-to-all-start.1) | async-done | bytes 65568 | tf_op jit(solution)/shard_map/all_to_all | solution.py:54
  29.2 0.1 reduce_sum.81
  29.3 0.4 subtract_select_fusion
  29.8 0.1 reduce_sum.83
  29.9 0.1 select_reduce_fusion
  30.0 0.2 convolution_add_fusion
  30.2 0.3 convolution_convert_fusion.2
  30.5 0.0 copy-start.6
  30.6 0.9 %reduce.13 = bf16[8,2048]{1,0:T(8,128)(2,1)S(1)} reduce(bf16[8,1,2048]{2,1,0:T(2,128)(2,1)S(1)} %broadcast_in_dim.84, bf16[]{:T(256)} %broadcast.188), dimensions={1}, to_apply=%broadcast_in_dim.84.reduce_sub_computation | reduce | bytes 65538 | tf_op jit(solution)/shard_map/broadcast_in_dim | solution.py:95
  31.4 0.6 reshape.342
  32.0 3.3 %all-to-all-start.2 = ((bf16[8,2,1024]{2,1,0:T(2,128)(2,1)}), bf16[8,2,1024]{2,1,0:T(2,128)(2,1)S(1)}, u32[]{:S(2)}, u32[]{:S(2)}) async-start(bf16[8,2,1024]{2,1,0:T(2,128)(2,1)} %reshape.342), calls=%async_computation.2 | async-start | bytes 65536 | tf_op jit(solution)/shard_map/all_to_all | solution.py:94
  35.4 0.1 copy.65
  35.5 6.5 %all-to-all-done.2 = bf16[8,2,1024]{2,1,0:T(2,128)(2,1)S(1)} async-done(((bf16[8,2,1024]{2,1,0:T(2,128)(2,1)}), bf16[8,2,1024]{2,1,0:T(2,128)(2,1)S(1)}, u32[]{:S(2)}, u32[]{:S(2)}) %all-to-all-start.2) | async-done | bytes 32800 | tf_op jit(solution)/shard_map/all_to_all | solution.py:94
  42.0 0.2 reduce.7
  42.3 0.2 fusion.2
  42.5 0.2 convolution_convert_fusion.1
  42.7 0.1 broadcast_in_dim.85
  42.7 0.1 all_to_all.41
  42.9 1.8 %reduce.14 = bf16[32,3072]{1,0:T(8,128)(2,1)S(1)} reduce(bf16[32,1,3072]{2,1,0:T(2,128)(2,1)S(1)} %all_to_all.41, bf16[]{:T(256)} %broadcast.188), dimensions={1}, to_apply=%all_to_all.41.reduce_sub_computation | reduce | bytes 393218 | tf_op jit(solution)/shard_map/all_to_all | solution.py:111
  44.7 0.8 %reshape.344 = bf16[32,2,1536]{2,1,0:T(2,128)(2,1)} reshape(bf16[32,3072]{1,0:T(8,128)(2,1)S(1)} %reduce.14) | data formatting | bytes 393216
  45.5 2.7 %all-to-all-start.3 = ((bf16[32,2,1536]{2,1,0:T(2,128)(2,1)}), bf16[32,2,1536]{2,1,0:T(2,128)(2,1)S(1)}, u32[]{:S(2)}, u32[]{:S(2)}) async-start(bf16[32,2,1536]{2,1,0:T(2,128)(2,1)} %reshape.344), calls=%async_computation.3 | async-start | bytes 393216 | tf_op jit(solution)/shard_map/all_to_all | solution.py:111
  48.2 0.0 copy-start.11
  48.2 0.6 copy-done.11
  48.9 0.6 convert_element_type.143
  49.4 7.7 %all-to-all-done.3 = bf16[32,2,1536]{2,1,0:T(2,128)(2,1)S(1)} async-done(((bf16[32,2,1536]{2,1,0:T(2,128)(2,1)}), bf16[32,2,1536]{2,1,0:T(2,128)(2,1)S(1)}, u32[]{:S(2)}, u32[]{:S(2)}) %all-to-all-start.3) | async-done | bytes 196640 | tf_op jit(solution)/shard_map/all_to_all | solution.py:111
  57.1 0.1 reshape.345
  57.3 1.1 %convert_reduce_fusion = f32[32,3072]{1,0:T(8,128)S(1)} fusion(bf16[32,1,3072]{2,1,0:T(2,128)(2,1)S(1)} %reshape.345), kind=kLoop, calls=%fused_computation.17 | loop fusion | flops 98304 | bytes 589824 | tf_op jit(solution)/shard_map/convert_element_type | solution.py:113
  58.4 0.1 reshape.333
  58.5 0.0 copy-start.3
  58.6 0.1 fusion.33
  58.7 0.7 multiply_convert_fusion
  59.4 0.1 copy-done.2
  59.5 0.3 fusion.9
  59.8 0.2 copy-done.4
  60.1 1.5 %fusion = bf16[8,1,2048]{2,0,1:T(8,128)(2,1)S(1)} fusion(bf16[8,2048]{1,0:T(8,128)(2,1)} %bitcast.69, bf16[1,192,2048]{2,1,0:T(8,128)(2,1)S(1)} %copy-done.3, bf16[1,2048,192]{1,2,0:T(8,128)(2,1)S(1)} %copy-done.4, f32[8,192]{1,0:T(8,128)S(1)} %fusion.9), kind=kOutput, calls=%fused_computation.1 | convolution fusion | flops 12608512 | bytes 1644544 | tf_op jit(solution)/shard_map/esf,efd->sed/dot_general | solution.py:121
  61.5 0.1 all_to_all.42
  61.6 0.8 %reduce.15 = bf16[32,512]{1,0:T(8,128)(2,1)S(1)} reduce(bf16[32,1,512]{2,1,0:T(2,128)(2,1)S(1)} %all_to_all.42, bf16[]{:T(256)} %broadcast.188), dimensions={1}, to_apply=%all_to_all.42.reduce_sub_computation | reduce | bytes 65538 | tf_op jit(solution)/shard_map/all_to_all | solution.py:125
  62.4 0.6 reshape.346
  63.0 2.7 %all-to-all-start.4 = ((bf16[32,2,256]{2,1,0:T(2,128)(2,1)}), bf16[32,2,256]{2,1,0:T(2,128)(2,1)S(1)}, u32[]{:S(2)}, u32[]{:S(2)}) async-start(bf16[32,2,256]{2,1,0:T(2,128)(2,1)} %reshape.346), calls=%async_computation.4 | async-start | bytes 65536 | tf_op jit(solution)/shard_map/all_to_all | solution.py:125
  65.7 0.0 copy-start.9
  65.7 0.7 copy-done.9
  66.4 0.1 select_reduce_fusion.1
  66.5 6.5 %all-to-all-done.4 = bf16[32,2,256]{2,1,0:T(2,128)(2,1)S(1)} async-done(((bf16[32,2,256]{2,1,0:T(2,128)(2,1)}), bf16[32,2,256]{2,1,0:T(2,128)(2,1)S(1)}, u32[]{:S(2)}, u32[]{:S(2)}) %all-to-all-start.4) | async-done | bytes 32800 | tf_op jit(solution)/shard_map/all_to_all | solution.py:125
  73.0 0.2 convert_reduce_fusion.1
  73.3 0.1 multiply_reduce_fusion
  73.4 0.6 add_convert_fusion
  (41 shorter events, 0.5 us)
Async XLA Ops:
  0.0 29.3 %copy-start = (bf16[4,1,1024,128]{3,2,1,0:T(8,128)(2,1)S(1)}, bf16[4,1,1024,128]{3,2,1,0:T(8,128)(2,1)}, u32[]{:S(2)}) copy-start(bf16[4,1,1024,128]{3,2,1,0:T(8,128)(2,1)} %param.19) | copy-start | bytes 3145732
  0.0 2.2 %copy-start.7 = (bf16[4,2048]{1,0:T(4,128)(2,1)S(1)}, bf16[4,2048]{1,0:T(4,128)(2,1)}, u32[]{:S(2)}) copy-start(bf16[4,2048]{1,0:T(4,128)(2,1)} %param.15) | copy-start | bytes 49156
  0.0 18.2 %copy-start.5 = (bf16[256,512]{1,0:T(8,128)(2,1)S(1)}, bf16[256,512]{1,0:T(8,128)(2,1)}, u32[]{:S(2)}) copy-start(bf16[256,512]{1,0:T(8,128)(2,1)} %param.17) | copy-start | bytes 786436
  4.1 13.9 %all-to-all-start = ((bf16[8,2,576]{2,1,0:T(2,128)(2,1)}), bf16[8,2,576]{2,1,0:T(2,128)(2,1)S(1)}, u32[]{:S(2)}, u32[]{:S(2)}) async-start(bf16[8,2,576]{2,1,0:T(2,128)(2,1)} %reshape.340), calls=%async_computation | async-start | bytes 40960 | tf_op jit(solution)/shard_map/all_to_all | solution.py:42
  18.3 11.9 %copy-start.1 = (bf16[4,1,1024,128]{3,2,1,0:T(8,128)(2,1)S(1)}, bf16[4,1,1024,128]{3,2,1,0:T(8,128)(2,1)}, u32[]{:S(2)}) copy-start(bf16[4,1,1024,128]{3,2,1,0:T(8,128)(2,1)} %param.20) | copy-start | bytes 3145732
  19.0 10.2 %all-to-all-start.1 = ((f32[8,1,2048]{2,1,0:T(1,128)}), f32[8,1,2048]{2,1,0:T(1,128)S(1)}, u32[]{:S(2)}, u32[]{:S(2)}) async-start(f32[8,1,2048]{2,1,0:T(1,128)} %all_to_all.40), calls=%async_computation.1 | async-start | bytes 131072 | tf_op jit(solution)/shard_map/all_to_all | solution.py:54
  30.5 11.7 %copy-start.6 = (bf16[512,256]{1,0:T(8,128)(2,1)S(1)}, bf16[512,256]{1,0:T(8,128)(2,1)}, u32[]{:S(2)}) copy-start(bf16[512,256]{1,0:T(8,128)(2,1)} %param.22) | copy-start | bytes 786436
  32.0 10.0 %all-to-all-start.2 = ((bf16[8,2,1024]{2,1,0:T(2,128)(2,1)}), bf16[8,2,1024]{2,1,0:T(2,128)(2,1)S(1)}, u32[]{:S(2)}, u32[]{:S(2)}) async-start(bf16[8,2,1024]{2,1,0:T(2,128)(2,1)} %reshape.342), calls=%async_computation.2 | async-start | bytes 65536 | tf_op jit(solution)/shard_map/all_to_all | solution.py:94
  45.5 2.7 %copy-start.8 = (f32[2048]{0:T(1024)S(1)}, f32[2048]{0:T(1024)}, u32[]{:S(2)}) copy-start(f32[2048]{0:T(1024)} %param.23) | copy-start | bytes 24580
  45.5 11.7 %all-to-all-start.3 = ((bf16[32,2,1536]{2,1,0:T(2,128)(2,1)}), bf16[32,2,1536]{2,1,0:T(2,128)(2,1)S(1)}, u32[]{:S(2)}, u32[]{:S(2)}) async-start(bf16[32,2,1536]{2,1,0:T(2,128)(2,1)} %reshape.344), calls=%async_computation.3 | async-start | bytes 393216 | tf_op jit(solution)/shard_map/all_to_all | solution.py:111
  48.2 0.7 copy-start.11
  58.4 1.1 %copy-start.2 = (bf16[1,2048,192]{1,2,0:T(8,128)(2,1)S(1)}, bf16[1,2048,192]{1,2,0:T(8,128)(2,1)}, u32[]{:S(2)}) copy-start(bf16[1,2048,192]{1,2,0:T(8,128)(2,1)} %param.27) | copy-start | bytes 2359300
  58.5 1.3 %copy-start.3 = (bf16[1,192,2048]{2,1,0:T(8,128)(2,1)S(1)}, bf16[1,192,2048]{2,1,0:T(8,128)(2,1)}, u32[]{:S(2)}) copy-start(bf16[1,192,2048]{2,1,0:T(8,128)(2,1)} %param.29) | copy-start | bytes 2359300
  58.6 1.5 %copy-start.4 = (bf16[1,2048,192]{1,2,0:T(8,128)(2,1)S(1)}, bf16[1,2048,192]{1,2,0:T(8,128)(2,1)}, u32[]{:S(2)}) copy-start(bf16[1,2048,192]{1,2,0:T(8,128)(2,1)} %param.28) | copy-start | bytes 2359300
  63.0 2.7 %copy-start.10 = (f32[4,2]{0,1:T(2,128)S(1)}, f32[4,2]{0,1:T(2,128)}, u32[]{:S(2)}) copy-start(f32[4,2]{0,1:T(2,128)} %convert_element_type.143) | copy-start | bytes 100
  63.0 10.0 %all-to-all-start.4 = ((bf16[32,2,256]{2,1,0:T(2,128)(2,1)}), bf16[32,2,256]{2,1,0:T(2,128)(2,1)S(1)}, u32[]{:S(2)}, u32[]{:S(2)}) async-start(bf16[32,2,256]{2,1,0:T(2,128)(2,1)} %reshape.346), calls=%async_computation.4 | async-start | bytes 65536 | tf_op jit(solution)/shard_map/all_to_all | solution.py:125
  65.7 0.7 copy-start.9

commit v2 on v1

--- a/solution.py
+++ b/solution.py
@@ -1,12 +1,261 @@
 import jax
 import jax.numpy as jnp
 from jax import lax
+from jax.experimental import pallas as pl
+from jax.experimental.pallas import tpu as pltpu
 from jax.sharding import PartitionSpec as P
 
 rms_epsilon = 1e-06
-
-
-def body(
+f32, bf16, i32 = jnp.float32, jnp.bfloat16, jnp.int32
+in_vmem = pl.BlockSpec(memory_space=pltpu.VMEM)
+in_smem = pl.BlockSpec(memory_space=pltpu.SMEM)
+
+
+def send_kernel(hidden_ref, group_ref, inner_ref, out_ref, *, group_size):
+    n_ep, height, rows = out_ref.shape
+    tokens, top_k = inner_ref.shape
+    lane = lax.broadcasted_iota(i32, (tokens, rows), 1)
+    ids = jnp.zeros((tokens, rows), f32)
+    for t in range(tokens):
+        for k in range(top_k):
+            value = (group_ref[t] * group_size + inner_ref[t, k]).astype(f32)
+            ids = jnp.where(lane == t * top_k + k, value, ids)
+    for e in range(n_ep):
+        part = hidden_ref[:, e * rows : (e + 1) * rows].astype(f32)
+        out_ref[e] = jnp.concatenate([part, ids], axis=0).astype(bf16)
+
+
+def query_kernel(features_ref, gain_ref, weight_ref, out_ref, *, tokens):
+    n_ep, height, rows = features_ref.shape
+    heads = out_ref.shape[1] // tokens
+    size = out_ref.shape[2]
+    gain = gain_ref[pl.ds(lax.axis_index("ep"), 1), :]
+    flat = features_ref[...].astype(f32).reshape(n_ep * height, rows)
+    parts = jnp.dot((flat * gain).astype(bf16), weight_ref[...], preferred_element_type=f32)
+    parts = parts.reshape(n_ep, height, heads * size)
+    for h in range(heads):
+        out_ref[:, h * tokens : (h + 1) * tokens, :] = parts[:, :tokens, h * size : (h + 1) * size]
+
+
+def attend_kernel(
+    parts_ref, hidden_ref, key_ref, value_ref, lengths_ref, bias_ref, out_ref
+):
+    tokens, _, cache, size = key_ref.shape
+    n_ep, rows, _ = parts_ref.shape
+    heads = rows // tokens
+    chunk = 128
+    wide = hidden_ref[...].astype(f32)
+    scale = lax.rsqrt(jnp.mean(wide * wide, axis=-1, keepdims=True) + rms_epsilon)
+    queries = jnp.sum(parts_ref[...], axis=0) * jnp.concatenate([scale] * heads, axis=0)
+    queries = queries.astype(bf16)
+    row = lax.broadcasted_iota(i32, (rows, 1), 0)
+    token_of, head_of = row % tokens, row // tokens
+    bias = jnp.zeros((rows, 1), f32)
+    first = lax.axis_index("tp") * heads
+    for h in range(heads):
+        bias = jnp.where(head_of == h, bias_ref[first + h], bias)
+    length = jnp.zeros((rows, 1), i32)
+    for t in range(tokens):
+        length = jnp.where(token_of == t, lengths_ref[t], length)
+    scores = jnp.zeros((rows, cache), f32)
+    for t in range(tokens):
+        found = lax.dot_general(
+            queries, key_ref[t, 0], (((1,), (1,)), ((), ())), preferred_element_type=f32
+        )
+        scores = jnp.where(token_of == t, found, scores)
+    scores = scores * size ** (-0.5) + bias
+    visible = lax.broadcasted_iota(i32, (rows, cache), 1) < length
+    soft = jnp.log1p(jnp.exp(-jnp.abs(scores)))
+    log_keep = jnp.where(visible, -jnp.maximum(scores, 0.0) - soft, 0.0)
+    log_take = jnp.minimum(scores, 0.0) - soft
+    count = cache // chunk
+    stacked = jnp.concatenate([log_keep[:, c * chunk : (c + 1) * chunk] for c in range(count)], axis=0)
+    later = (
+        lax.broadcasted_iota(i32, (chunk, chunk), 0) > lax.broadcasted_iota(i32, (chunk, chunk), 1)
+    ).astype(f32)
+    inner = jnp.dot(stacked, later, preferred_element_type=f32, precision=lax.Precision.HIGHEST)
+    totals = jnp.sum(stacked, axis=1, keepdims=True)
+    running = jnp.zeros((rows, 1), f32)
+    pieces = [None] * count
+    for c in reversed(range(count)):
+        pieces[c] = inner[c * rows : (c + 1) * rows] + running
+        running = running + totals[c * rows : (c + 1) * rows]
+    later_sum = jnp.concatenate(pieces, axis=1)
+    weight = jnp.where(visible, jnp.exp(log_take + later_sum), 0.0).astype(bf16)
+    result = jnp.zeros((rows, size), f32)
+    for t in range(tokens):
+        found = jnp.dot(weight, value_ref[t, 0], preferred_element_type=f32)
+        result = jnp.where(token_of == t, found, result)
+    result = result.astype(bf16)
+    for e in range(n_ep):
+        out_ref[e] = result
+
+
+def project_kernel(heads_ref, weight_ref, features_ref, pick_ref, out_ref, *, tokens, n_tp):
+    n_ep, rows, size = heads_ref.shape
+    heads = rows // tokens
+    height, columns = features_ref.shape[1:]
+    flat = heads_ref[...].reshape(n_ep * rows, size)
+    total = features_ref[...].astype(f32) * (1.0 / n_tp)
+    total = total[:, :tokens, :]
+    for h in range(heads):
+        found = jnp.dot(
+            flat, weight_ref[h * size : (h + 1) * size, :], preferred_element_type=f32
+        ).reshape(n_ep, rows, columns)
+        total = total + found[:, h * tokens : (h + 1) * tokens, :]
+    total = jnp.concatenate([total, jnp.zeros((n_ep, height - tokens, columns), f32)], axis=1)
+    total = total.reshape(n_ep * height, columns).astype(bf16)
+    message = jnp.dot(pick_ref[...], total, preferred_element_type=f32).astype(bf16)
+    message = message.reshape(n_ep, out_ref.shape[2], columns)
+    for g in range(n_tp):
+        out_ref[:, g] = message
+
+
+def expert_kernel(parts_ref, gain_ref, gate_ref, up_ref, down_ref, out_ref, own_ref, *, tokens):
+    n_ep, n_tp, height, columns = parts_ref.shape
+    size = out_ref.shape[2]
+    pieces = []
+    for e in range(n_ep):
+        piece = parts_ref[e, 0].astype(f32)
+        for g in range(1, n_tp):
+            piece = piece + parts_ref[e, g].astype(f32)
+        pieces.append(piece)
+    residual = jnp.concatenate(pieces, axis=1)
+    own_ref[...] = residual[n_ep:, :]
+    arrived = residual[:n_ep, :]
+    arrived = arrived * lax.rsqrt(jnp.mean(arrived * arrived, axis=-1, keepdims=True) + rms_epsilon)
+    arrived = (arrived * gain_ref[...]).astype(bf16)
+    gated = jnp.dot(arrived, gate_ref[0], preferred_element_type=f32)
+    up = jnp.dot(arrived, up_ref[0], preferred_element_type=f32)
+    active = (gated / (1.0 + jnp.exp(-gated)) * up).astype(bf16)
+    down = jnp.dot(active, down_ref[0], preferred_element_type=f32)
+    for j in range(out_ref.shape[1]):
+        out_ref[:, j, :] = down[:, j * size : (j + 1) * size]
+
+
+def fast_body(
+    hidden,
+    attn_gain,
+    query_weight,
+    head_bias,
+    key_cache,
+    value_cache,
+    lengths,
+    out_weight,
+    moe_gain,
+    route_group,
+    route_inner,
+    route_weight,
+    gate_w,
+    up_w,
+    down_w,
+):
+    n_tp = lax.axis_size("tp")
+    n_ep = lax.axis_size("ep")
+    tokens, d_model = hidden.shape
+    rows, width = query_weight.shape
+    columns = out_weight.shape[1]
+    size = key_cache.shape[3]
+    heads = width // size
+    experts = n_ep
+    group_size = experts // max(2, experts // 32)
+    top_k = route_inner.shape[1]
+    height = 2 * tokens
+    part_width = d_model // n_tp
+    call = pl.pallas_call
+
+    packed = call(
+        lambda *refs: send_kernel(*refs, group_size=group_size),
+        name="send",
+        out_shape=jax.ShapeDtypeStruct((n_ep, height, rows), bf16),
+        in_specs=[in_vmem, in_smem, in_smem],
+        out_specs=in_vmem,
+    )(hidden, route_group, route_inner)
+    packed = lax.all_to_all(packed, "ep", split_axis=0, concat_axis=0, tiled=True)
+
+    parts = call(
+        lambda *refs: query_kernel(*refs, tokens=tokens),
+        name="query",
+        out_shape=jax.ShapeDtypeStruct((n_ep, heads * tokens, size), f32),
+        in_specs=[in_vmem] * 3,
+        out_specs=in_vmem,
+    )(packed, attn_gain.reshape(n_ep, rows), query_weight)
+    parts = lax.all_to_all(parts, "ep", split_axis=0, concat_axis=0, tiled=True)
+
+    heads_out = call(
+        attend_kernel,
+        name="attend",
+        out_shape=jax.ShapeDtypeStruct((n_ep, heads * tokens, size), bf16),
+        in_specs=[in_vmem] * 4 + [in_smem] * 2,
+        out_specs=in_vmem,
+    )(parts, hidden, key_cache, value_cache, lengths, head_bias)
+    heads_out = lax.all_to_all(heads_out, "ep", split_axis=0, concat_axis=0, tiled=True)
+
+    named = packed[:, tokens, : tokens * top_k].reshape(n_ep, tokens, top_k).astype(i32)
+    named = jnp.pad(named, ((0, 0), (0, height - tokens), (0, 0)), constant_values=-1)
+    named = named.reshape(1, 1, n_ep, height, top_k)
+    message_rows = -(-(n_ep + tokens) // 16) * 16
+    shape = (n_ep, message_rows, n_ep, height)
+    expert = lax.broadcasted_iota(i32, shape, 0)
+    slot = lax.broadcasted_iota(i32, shape, 1)
+    block = lax.broadcasted_iota(i32, shape, 2)
+    place = lax.broadcasted_iota(i32, shape, 3)
+    hit = jnp.any(named == expert[..., None], axis=-1)
+    pick = ((slot == block) & hit) | ((block == expert) & (slot == n_ep + place) & (place < tokens))
+    pick = pick.astype(bf16).reshape(n_ep * message_rows, n_ep * height)
+
+    message = call(
+        lambda *refs: project_kernel(*refs, tokens=tokens, n_tp=n_tp),
+        name="project",
+        out_shape=jax.ShapeDtypeStruct((n_ep, n_tp, message_rows, columns), bf16),
+        in_specs=[in_vmem] * 4,
+        out_specs=in_vmem,
+    )(heads_out, out_weight, packed, pick)
+    message = message.reshape(n_ep * n_tp, message_rows, columns)
+    message = lax.all_to_all(message, ("ep", "tp"), split_axis=0, concat_axis=0, tiled=True)
+
+    down_out, own = call(
+        lambda *refs: expert_kernel(*refs, tokens=tokens),
+        name="expert",
+        out_shape=(
+            jax.ShapeDtypeStruct((n_ep, d_model // size, size), f32),
+            jax.ShapeDtypeStruct((message_rows - n_ep, d_model), f32),
+        ),
+        in_specs=[in_vmem] * 5,
+        out_specs=(in_vmem, in_vmem),
+    )(
+        message.reshape(n_ep, n_tp, message_rows, columns),
+        moe_gain.reshape(1, d_model),
+        gate_w,
+        up_w,
+        down_w,
+    )
+    lanes = part_width // size
+    returned = lax.all_to_all(
+        down_out.reshape(n_ep * n_tp, lanes, size), ("ep", "tp"), split_axis=0, concat_axis=0, tiled=True
+    )
+    returned = returned.reshape(n_ep, n_tp, lanes, size).sum(axis=1)
+    chosen = route_group[:, None] * group_size + route_inner
+    matches = chosen[:, :, None] == jnp.arange(experts, dtype=i32)[None, None, :]
+    mixing = jnp.sum(jnp.where(matches, route_weight[:, :, None].astype(f32), 0.0), axis=1)
+    mixed = jnp.sum(mixing[:, :, None, None] * returned[None], axis=1).reshape(tokens, part_width)
+    own = lax.dynamic_slice_in_dim(own[:tokens], lax.axis_index("tp") * part_width, part_width, 1)
+    return (own + mixed).astype(bf16)
+
+
+def body(*args):
+    hidden, query_weight, key_cache = args[0], args[2], args[4]
+    out_weight, gate_w = args[7], args[12]
+    aligned = all(
+        extent % 128 == 0
+        for extent in (query_weight.shape[0], query_weight.shape[1], out_weight.shape[1])
+    )
+    single = gate_w.shape[0] == 1 and key_cache.shape[1] == 1
+    shapes = hidden.shape[0] == 4 and key_cache.shape[3] == 128 and key_cache.shape[2] % 128 == 0
+    return fast_body(*args) if aligned and single and shapes else plain_body(*args)
+
+
+def plain_body(
     hidden,
     attn_gain,
     query_weight,

time: 74.7 us -> 74.5 us (level)
  Pallas kernels: 0 us -> 11.7 us
  other arithmetic: 11 us -> 1.69 us
  matrix products: 3.17 us -> 0 us
    pallas_call x0 -> x5, Pallas kernels: none -> 11.7 us  [the longest x1 3.26 us: fast_body(): call(attend_kernel, name='attend', out_shape=jax.ShapeDtypeStruct((n_ep,...]
    all_to_all x5 -> x0, other arithmetic: 3.41 us -> none  [the longest x1 1.77 us: body(): lax.all_to_all(message, ('ep', 'tp'), split_axis=0, concat_axis=0, tiled=...]
    dot_general x8 -> x0, matrix products: 3.17 us -> none  [the longest x1 1.45 us: body(): jnp.einsum('esf,efd->sed', activated, down_w, preferred_element_type=f32)]
    convert_element_type x8 -> x3, other arithmetic: 4.38 us -> 1.33 us  [the longest x1 0.72 us: fast_body(): pick = pick.astype(bf16).reshape(n_ep * message_rows, n_ep * height)]
    unnamed x34 -> x25, local copies, waits for them, and re-layouts: 4.71 us -> 7.41 us
    dynamic_slice x2 -> x0, local copies, waits for them, and re-layouts: 1.49 us -> none  [the longest x1 0.76 us: body(): gain_block = lax.dynamic_slice_in_dim(attn_gain, ep_index * rows, rows, 0)]
    all_to_all x4 -> x0, local copies, waits for them, and re-layouts: 1.45 us -> none  [the longest x1 0.7 us: body(): lax.all_to_all(parts.reshape(n_ep, tokens * width), 'ep', split_axis=0, c...]
    broadcast_in_dim x1 -> x0, other arithmetic: 0.86 us -> none  [body(): jnp.broadcast_to(heads_out, (n_ep, tokens * width))]
  transfers between devices with their start and end apart: 5 -> 5, of which waited for: 5 -> 5; matrix products, arithmetic and copies ran while one was open for 4% -> 7% of each run, Pallas kernels for 0% -> 0%
where the time goes in v2:
time: 74.5 us; the launch traced here: 73.8 us
  waiting for transfers between devices  32 us (43%)
  starting transfers between devices  19.3 us (26%)
  Pallas kernels  11.7 us (16%)
  local copies, waits for them, and re-layouts  8.97 us (12%)
  other arithmetic  1.69 us (2%)
    all_to_all x1, waiting for transfers between devices, fast_body(): lax.all_to_all(message, ('ep', 'tp'), split_axis=0, concat_axis=0, tiled=...  7.96 us
    unnamed x25, local copies, waits for them, and re-layouts  7.41 us
    all_to_all x1, starting transfers between devices, fast_body(): lax.all_to_all(packed, 'ep', split_axis=0, concat_axis=0, tiled=True)  7.28 us
    all_to_all x1, waiting for transfers between devices, fast_body(): lax.all_to_all(down_out.reshape(n_ep * n_tp, lanes, size), ('ep', 'tp'),...  6.63 us
    all_to_all x1, waiting for transfers between devices, fast_body(): parts = lax.all_to_all(parts, 'ep', split_axis=0, concat_axis=0, tiled=True)  6.35 us
    all_to_all x1, waiting for transfers between devices, fast_body(): lax.all_to_all(heads_out, 'ep', split_axis=0, concat_axis=0, tiled=True)  5.9 us
    all_to_all x1, waiting for transfers between devices, fast_body(): lax.all_to_all(packed, 'ep', split_axis=0, concat_axis=0, tiled=True)  5.11 us
    all_to_all x1, starting transfers between devices, fast_body(): lax.all_to_all(heads_out, 'ep', split_axis=0, concat_axis=0, tiled=True)  3.47 us
  transfers between devices with their start and end apart: 5, of which 5 were waited for; matrix products, arithmetic and copies ran while one was open for 7% of the time, Pallas kernels for 0%

profile of v2, /device:TPU:0, one launch (start us, length us, event | category | flops | bytes accessed | tf_op | source)
XLA Modules:
  0.0 73.8 jit_solution(16791864497172740871)
XLA Ops:
  0.0 1.3 %copy.46.refs_2_ = s32[4,2]{1,0:T(4,128)} copy(s32[4,2]{0,1:T(2,128)} %param.25) | data formatting | bytes 64 | tf_op args[10]
  1.3 1.5 %send.1 = bf16[8,8,256]{2,1,0:T(8,128)(2,1)} custom-call(bf16[4,2048]{1,0:T(4,128)(2,1)} %hidden_ref.1, s32[4]{0:T(128)} %refs_1_.2, s32[4,2]{1,0:T(4,128)} %copy.46.refs_2_), custom_call_target="tpu_custom_call" | custom-call | tf_op jit(solution)/shard_map/send/pallas_call | solution.py:167
  2.8 7.3 %all-to-all-start = ((bf16[8,8,256]{2,1,0:T(8,128)(2,1)}), bf16[8,8,256]{2,1,0:T(8,128)(2,1)S(1)}, u32[]{:S(2)}, u32[]{:S(2)}) async-start(bf16[8,8,256]{2,1,0:T(8,128)(2,1)} %send.1), calls=%async_computation | async-start | bytes 65536 | tf_op jit(solution)/shard_map/all_to_all | solution.py:174
  10.1 0.1 iota.83
  10.2 0.1 iota.73
  10.3 0.1 iota.76
  10.3 0.0 copy-start.7
  10.4 0.1 iota.79
  10.5 0.1 iota.86
  10.5 0.5 copy-done.7
  11.1 0.6 reshape.41.refs_1_
  11.7 5.1 %all-to-all-done.refs_0_.refs_2_ = bf16[8,8,256]{2,1,0:T(8,128)(2,1)S(1)} async-done(((bf16[8,8,256]{2,1,0:T(8,128)(2,1)}), bf16[8,8,256]{2,1,0:T(8,128)(2,1)S(1)}, u32[]{:S(2)}, u32[]{:S(2)}) %all-to-all-start) | async-done | bytes 32800 | tf_op jit(solution)/shard_map/all_to_all | solution.py:174
  16.8 0.0 copy-start.3
  16.8 0.1 copy.48
  16.9 0.1 copy.49
  17.0 0.4 copy-done.3
  17.4 1.8 %query.1 = f32[8,16,128]{2,1,0:T(8,128)} custom-call(bf16[8,8,256]{2,1,0:T(8,128)(2,1)} %copy-done.3, f32[8,256]{1,0:T(8,128)} %reshape.41.refs_1_, bf16[256,512]{1,0:T(8,128)(2,1)} %refs_2_.3), custom_call_target="tpu_custom_call" | custom-call | tf_op jit(solution)/shard_map/query/pallas_call | solution.py:176
  19.2 3.3 %all-to-all-start.1 = ((f32[8,16,128]{2,1,0:T(8,128)}), f32[8,16,128]{2,1,0:T(8,128)S(1)}, u32[]{:S(2)}, u32[]{:S(2)}) async-start(f32[8,16,128]{2,1,0:T(8,128)} %query.1), calls=%async_computation.1 | async-start | bytes 131072 | tf_op jit(solution)/shard_map/all_to_all | solution.py:183
  22.5 0.1 fusion
  22.7 0.1 reduce_or.12
  22.9 0.1 copy.52
  23.0 6.3 %all-to-all-done.1.parts_ref = f32[8,16,128]{2,1,0:T(8,128)S(1)} async-done(((f32[8,16,128]{2,1,0:T(8,128)}), f32[8,16,128]{2,1,0:T(8,128)S(1)}, u32[]{:S(2)}, u32[]{:S(2)}) %all-to-all-start.1) | async-done | bytes 65568 | tf_op jit(solution)/shard_map/all_to_all | solution.py:183
  29.4 0.0 copy-start.4
  29.4 0.6 copy-done.4
  30.0 3.3 %attend.1 = bf16[8,16,128]{2,1,0:T(8,128)(2,1)} custom-call(f32[8,16,128]{2,1,0:T(8,128)} %copy-done.4, bf16[4,2048]{1,0:T(4,128)(2,1)} %hidden_ref.1, bf16[4,1,1024,128]{3,2,1,0:T(8,128)(2,1)} %key_ref.1, bf16[4,1,1024,128]{3,2,1,0:T(8,128)(2,1)} %value_ref.1, s32[4]{0:T(128)} %lengths_ref.1, f32[16]{0:T(128)} %bias_ref.1), custom_call_target="tpu_custom_call" | custom-call | tf_op jit(solution)/shard_map/attend/pallas_call | solution.py:185
  33.3 0.0 copy-start.1
  33.3 3.5 %all-to-all-start.2 = ((bf16[8,16,128]{2,1,0:T(8,128)(2,1)}), bf16[8,16,128]{2,1,0:T(8,128)(2,1)S(1)}, u32[]{:S(2)}, u32[]{:S(2)}) async-start(bf16[8,16,128]{2,1,0:T(8,128)(2,1)} %attend.1), calls=%async_computation.2 | async-start | bytes 65536 | tf_op jit(solution)/shard_map/all_to_all | solution.py:192
  36.7 0.7 or_convert_fusion.refs_3_
  37.5 5.9 %all-to-all-done.2.refs_0_ = bf16[8,16,128]{2,1,0:T(8,128)(2,1)S(1)} async-done(((bf16[8,16,128]{2,1,0:T(8,128)(2,1)}), bf16[8,16,128]{2,1,0:T(8,128)(2,1)S(1)}, u32[]{:S(2)}, u32[]{:S(2)}) %all-to-all-start.2) | async-done | bytes 32800 | tf_op jit(solution)/shard_map/all_to_all | solution.py:192
  43.4 0.0 copy-start.5
  43.4 0.6 copy-done.5
  44.0 2.0 %project.1 = bf16[8,4,16,256]{3,2,1,0:T(8,128)(2,1)} custom-call(bf16[8,16,128]{2,1,0:T(8,128)(2,1)} %copy-done.5, bf16[512,256]{1,0:T(8,128)(2,1)} %refs_1_.3, bf16[8,8,256]{2,1,0:T(8,128)(2,1)} %copy-done.3, bf16[128,64]{1,0:T(8,128)(2,1)} %or_convert_fusion.refs_3_), custom_call_target="tpu_custom_call" | custom-call | tf_op jit(solution)/shard_map/project/pallas_call | solution.py:207
  46.0 2.6 %all-to-all-start.3 = ((bf16[32,16,256]{2,1,0:T(8,128)(2,1)}), bf16[32,16,256]{2,1,0:T(8,128)(2,1)S(1)}, u32[]{:S(2)}, u32[]{:S(2)}) async-start(bf16[32,16,256]{2,1,0:T(8,128)(2,1)} %bitcast.17), calls=%async_computation.3 | async-start | bytes 524288 | tf_op jit(solution)/shard_map/all_to_all | solution.py:215
  48.6 0.0 copy-done.1
  48.6 0.0 copy-start.2
  48.6 1.3 %copy.54.refs_2_ = bf16[1,2048,192]{2,1,0:T(8,128)(2,1)} copy(bf16[1,2048,192]{1,2,0:T(8,128)(2,1)S(1)} %copy-done.1) | data formatting | bytes 1572864 | tf_op args[12]
  49.9 0.0 copy-done.2
  49.9 0.0 copy-start.9
  49.9 1.3 %copy.55.refs_3_ = bf16[1,2048,192]{2,1,0:T(8,128)(2,1)} copy(bf16[1,2048,192]{1,2,0:T(8,128)(2,1)S(1)} %copy-done.2) | data formatting | bytes 1572864 | tf_op args[13]
  51.2 0.0 copy-done.9
  51.2 8.0 %all-to-all-done.3 = bf16[32,16,256]{2,1,0:T(8,128)(2,1)S(1)} async-done(((bf16[32,16,256]{2,1,0:T(8,128)(2,1)}), bf16[32,16,256]{2,1,0:T(8,128)(2,1)S(1)}, u32[]{:S(2)}, u32[]{:S(2)}) %all-to-all-start.3) | async-done | bytes 262176 | tf_op jit(solution)/shard_map/all_to_all | solution.py:215
  59.2 0.0 copy-start
  59.2 0.7 copy-done
  59.9 3.2 %expert.1 = (f32[8,16,128]{2,1,0:T(8,128)}, f32[8,2048]{1,0:T(8,128)}) custom-call(bf16[8,4,16,256]{3,2,1,0:T(8,128)(2,1)} %bitcast.16, f32[1,2048]{1,0:T(1,128)} %bitcast.20, bf16[1,2048,192]{2,1,0:T(8,128)(2,1)} %copy.54.refs_2_, bf16[1,2048,192]{2,1,0:T(8,128)(2,1)} %copy.55.refs_3_, bf16[1,192,2048]{2,1,0:T(8,128)(2,1)} %refs_4_.1), custom_call_target="tpu_custom_call" | custom-call | tf_op jit(solution)/shard_map/expert/pallas_call | solution.py:217
  63.0 0.0 copy-start.8
  63.0 0.0 copy-start.6
  63.0 2.7 %all-to-all-start.4 = ((f32[32,4,128]{2,1,0:T(4,128)}), f32[32,4,128]{2,1,0:T(4,128)S(1)}, u32[]{:S(2)}, u32[]{:S(2)}) async-start(f32[32,4,128]{2,1,0:T(4,128)} %bitcast.18), calls=%async_computation.4 | async-start | bytes 131072 | tf_op jit(solution)/shard_map/all_to_all | solution.py:234
  65.7 0.0 copy-done.8
  65.7 0.0 copy-start.10
  65.7 0.6 copy-done.10
  66.4 0.1 select_reduce_fusion
  66.5 0.0 copy-done.6
  66.5 6.6 %all-to-all-done.4 = f32[32,4,128]{2,1,0:T(4,128)S(1)} async-done(((f32[32,4,128]{2,1,0:T(4,128)}), f32[32,4,128]{2,1,0:T(4,128)S(1)}, u32[]{:S(2)}, u32[]{:S(2)}) %all-to-all-start.4) | async-done | bytes 65568 | tf_op jit(solution)/shard_map/all_to_all | solution.py:234
  73.1 0.1 multiply_reduce_fusion
  73.2 0.6 fusion.1
  (17 shorter events, 0.1 us)
Async XLA Ops:
  2.8 14.0 %all-to-all-start = ((bf16[8,8,256]{2,1,0:T(8,128)(2,1)}), bf16[8,8,256]{2,1,0:T(8,128)(2,1)S(1)}, u32[]{:S(2)}, u32[]{:S(2)}) async-start(bf16[8,8,256]{2,1,0:T(8,128)(2,1)} %send.1), calls=%async_computation | async-start | bytes 65536 | tf_op jit(solution)/shard_map/all_to_all | solution.py:174
  10.3 0.7 copy-start.7
  16.8 0.6 copy-start.3
  19.2 10.2 %all-to-all-start.1 = ((f32[8,16,128]{2,1,0:T(8,128)}), f32[8,16,128]{2,1,0:T(8,128)S(1)}, u32[]{:S(2)}, u32[]{:S(2)}) async-start(f32[8,16,128]{2,1,0:T(8,128)} %query.1), calls=%async_computation.1 | async-start | bytes 131072 | tf_op jit(solution)/shard_map/all_to_all | solution.py:183
  29.4 0.6 copy-start.4
  33.3 15.3 %copy-start.1 = (bf16[1,2048,192]{1,2,0:T(8,128)(2,1)S(1)}, bf16[1,2048,192]{1,2,0:T(8,128)(2,1)}, u32[]{:S(2)}) copy-start(bf16[1,2048,192]{1,2,0:T(8,128)(2,1)} %param.27) | copy-start | bytes 2359300
  33.3 10.1 %all-to-all-start.2 = ((bf16[8,16,128]{2,1,0:T(8,128)(2,1)}), bf16[8,16,128]{2,1,0:T(8,128)(2,1)S(1)}, u32[]{:S(2)}, u32[]{:S(2)}) async-start(bf16[8,16,128]{2,1,0:T(8,128)(2,1)} %attend.1), calls=%async_computation.2 | async-start | bytes 65536 | tf_op jit(solution)/shard_map/all_to_all | solution.py:192
  43.4 0.6 copy-start.5
  46.0 13.2 %all-to-all-start.3 = ((bf16[32,16,256]{2,1,0:T(8,128)(2,1)}), bf16[32,16,256]{2,1,0:T(8,128)(2,1)S(1)}, u32[]{:S(2)}, u32[]{:S(2)}) async-start(bf16[32,16,256]{2,1,0:T(8,128)(2,1)} %bitcast.17), calls=%async_computation.3 | async-start | bytes 524288 | tf_op jit(solution)/shard_map/all_to_all | solution.py:215
  48.6 1.3 %copy-start.2 = (bf16[1,2048,192]{1,2,0:T(8,128)(2,1)S(1)}, bf16[1,2048,192]{1,2,0:T(8,128)(2,1)}, u32[]{:S(2)}) copy-start(bf16[1,2048,192]{1,2,0:T(8,128)(2,1)} %param.28) | copy-start | bytes 2359300
  49.9 1.3 %copy-start.9 = (s32[4]{0:T(128)S(1)}, s32[4]{0:T(128)}, u32[]{:S(2)}) copy-start(s32[4]{0:T(128)} %refs_1_.2) | copy-start | bytes 52
  59.2 0.7 copy-start
  63.0 2.7 %copy-start.8 = (s32[4,2]{0,1:T(2,128)S(1)}, s32[4,2]{0,1:T(2,128)}, u32[]{:S(2)}) copy-start(s32[4,2]{0,1:T(2,128)} %param.25) | copy-start | bytes 100
  63.0 3.4 %copy-start.6 = (f32[8,2048]{1,0:T(8,128)S(1)}, f32[8,2048]{1,0:T(8,128)}, u32[]{:S(2)}) copy-start(f32[8,2048]{1,0:T(8,128)} %get-tuple-element.7) | copy-start | bytes 196612
  63.0 10.1 %all-to-all-start.4 = ((f32[32,4,128]{2,1,0:T(4,128)}), f32[32,4,128]{2,1,0:T(4,128)S(1)}, u32[]{:S(2)}, u32[]{:S(2)}) async-start(f32[32,4,128]{2,1,0:T(4,128)} %bitcast.18), calls=%async_computation.4 | async-start | bytes 131072 | tf_op jit(solution)/shard_map/all_to_all | solution.py:234
  65.7 0.7 copy-start.10

commit v3 on v2

--- a/solution.py
+++ b/solution.py
@@ -11,14 +11,21 @@
 in_smem = pl.BlockSpec(memory_space=pltpu.SMEM)
 
 
+params = pltpu.CompilerParams(vmem_limit_bytes=24 * 1024 * 1024)
+
+
+def near(array):
+    return pltpu.with_memory_space_constraint(array, pltpu.VMEM)
+
+
 def send_kernel(hidden_ref, group_ref, inner_ref, out_ref, *, group_size):
     n_ep, height, rows = out_ref.shape
-    tokens, top_k = inner_ref.shape
+    top_k, tokens = inner_ref.shape
     lane = lax.broadcasted_iota(i32, (tokens, rows), 1)
     ids = jnp.zeros((tokens, rows), f32)
     for t in range(tokens):
         for k in range(top_k):
-            value = (group_ref[t] * group_size + inner_ref[t, k]).astype(f32)
+            value = (group_ref[t] * group_size + inner_ref[k, t]).astype(f32)
             ids = jnp.where(lane == t * top_k + k, value, ids)
     for e in range(n_ep):
         part = hidden_ref[:, e * rows : (e + 1) * rows].astype(f32)
@@ -29,7 +36,8 @@
     n_ep, height, rows = features_ref.shape
     heads = out_ref.shape[1] // tokens
     size = out_ref.shape[2]
-    gain = gain_ref[pl.ds(lax.axis_index("ep"), 1), :]
+    start = pl.multiple_of(lax.axis_index("ep") * rows, 128)
+    gain = gain_ref[:, pl.ds(start, rows)]
     flat = features_ref[...].astype(f32).reshape(n_ep * height, rows)
     parts = jnp.dot((flat * gain).astype(bf16), weight_ref[...], preferred_element_type=f32)
     parts = parts.reshape(n_ep, height, heads * size)
@@ -38,9 +46,13 @@
 
 
 def attend_kernel(
-    parts_ref, hidden_ref, key_ref, value_ref, lengths_ref, bias_ref, out_ref
+    parts_ref, hidden_ref, keys_ref, values_ref, lengths_ref, bias_ref, out_ref, key_ref, value_ref, sems
 ):
     tokens, _, cache, size = key_ref.shape
+    loads = [pltpu.make_async_copy(keys_ref.at[t], key_ref.at[t], sems.at[0, t]) for t in range(tokens)]
+    loads += [pltpu.make_async_copy(values_ref.at[t], value_ref.at[t], sems.at[1, t]) for t in range(tokens)]
+    for load in loads:
+        load.start()
     n_ep, rows, _ = parts_ref.shape
     heads = rows // tokens
     chunk = 128
@@ -59,6 +71,7 @@
         length = jnp.where(token_of == t, lengths_ref[t], length)
     scores = jnp.zeros((rows, cache), f32)
     for t in range(tokens):
+        loads[t].wait()
         found = lax.dot_general(
             queries, key_ref[t, 0], (((1,), (1,)), ((), ())), preferred_element_type=f32
         )
@@ -84,11 +97,36 @@
     weight = jnp.where(visible, jnp.exp(log_take + later_sum), 0.0).astype(bf16)
     result = jnp.zeros((rows, size), f32)
     for t in range(tokens):
+        loads[tokens + t].wait()
         found = jnp.dot(weight, value_ref[t, 0], preferred_element_type=f32)
         result = jnp.where(token_of == t, found, result)
     result = result.astype(bf16)
     for e in range(n_ep):
         out_ref[e] = result
+
+
+def pick_kernel(packed_ref, out_ref, *, tokens, top_k):
+    n_ep, height, rows = packed_ref.shape
+    shape = out_ref.shape
+    message_rows = shape[0] // n_ep
+    ids = packed_ref[...].astype(f32)[:, tokens, :]
+    lane = lax.broadcasted_iota(i32, (rows, shape[1]), 0)
+    column = lax.broadcasted_iota(i32, (rows, shape[1]), 1)
+    owner = lax.broadcasted_iota(i32, (n_ep, shape[1]), 0)
+    column_block = lax.broadcasted_iota(i32, (n_ep, shape[1]), 1) // height
+    row = lax.broadcasted_iota(i32, shape, 0)
+    expert, slot = row // message_rows, row % message_rows
+    place = lax.broadcasted_iota(i32, shape, 1)
+    block, place = place // height, place % height
+    hit = jnp.zeros(shape, jnp.bool_)
+    for k in range(top_k):
+        spread = (lane == (column % height) * top_k + k).astype(f32)
+        found = jnp.dot(ids, spread, preferred_element_type=f32, precision=lax.Precision.HIGHEST)
+        found = jnp.sum(jnp.where(owner == column_block, found, 0.0), axis=0, keepdims=True)
+        hit = hit | (found == expert.astype(f32))
+    routed = (slot == block) & hit
+    own = (block == expert) & (slot == n_ep + place)
+    out_ref[...] = ((routed | own) & (place < tokens)).astype(f32).astype(bf16)
 
 
 def project_kernel(heads_ref, weight_ref, features_ref, pick_ref, out_ref, *, tokens, n_tp):
@@ -125,8 +163,9 @@
     arrived = residual[:n_ep, :]
     arrived = arrived * lax.rsqrt(jnp.mean(arrived * arrived, axis=-1, keepdims=True) + rms_epsilon)
     arrived = (arrived * gain_ref[...]).astype(bf16)
-    gated = jnp.dot(arrived, gate_ref[0], preferred_element_type=f32)
-    up = jnp.dot(arrived, up_ref[0], preferred_element_type=f32)
+    across = (((1,), (1,)), ((), ()))
+    gated = lax.dot_general(arrived, gate_ref[0], across, preferred_element_type=f32)
+    up = lax.dot_general(arrived, up_ref[0], across, preferred_element_type=f32)
     active = (gated / (1.0 + jnp.exp(-gated)) * up).astype(bf16)
     down = jnp.dot(active, down_ref[0], preferred_element_type=f32)
     for j in range(out_ref.shape[1]):
@@ -170,7 +209,8 @@
         out_shape=jax.ShapeDtypeStruct((n_ep, height, rows), bf16),
         in_specs=[in_vmem, in_smem, in_smem],
         out_specs=in_vmem,
-    )(hidden, route_group, route_inner)
+        compiler_params=params,
+    )(hidden, route_group, route_inner.T)
     packed = lax.all_to_all(packed, "ep", split_axis=0, concat_axis=0, tiled=True)
 
     parts = call(
@@ -179,30 +219,34 @@
         out_shape=jax.ShapeDtypeStruct((n_ep, heads * tokens, size), f32),
         in_specs=[in_vmem] * 3,
         out_specs=in_vmem,
-    )(packed, attn_gain.reshape(n_ep, rows), query_weight)
+        compiler_params=params,
+    )(near(packed), near(attn_gain.reshape(1, d_model)), near(query_weight))
     parts = lax.all_to_all(parts, "ep", split_axis=0, concat_axis=0, tiled=True)
 
     heads_out = call(
         attend_kernel,
         name="attend",
         out_shape=jax.ShapeDtypeStruct((n_ep, heads * tokens, size), bf16),
-        in_specs=[in_vmem] * 4 + [in_smem] * 2,
+        in_specs=[in_vmem] * 2 + [pl.BlockSpec(memory_space=pl.ANY)] * 2 + [in_smem] * 2,
         out_specs=in_vmem,
-    )(parts, hidden, key_cache, value_cache, lengths, head_bias)
+        scratch_shapes=[
+            pltpu.VMEM(key_cache.shape, key_cache.dtype),
+            pltpu.VMEM(value_cache.shape, value_cache.dtype),
+            pltpu.SemaphoreType.DMA((2, tokens)),
+        ],
+        compiler_params=params,
+    )(near(parts), near(hidden), key_cache, value_cache, lengths, head_bias)
     heads_out = lax.all_to_all(heads_out, "ep", split_axis=0, concat_axis=0, tiled=True)
 
-    named = packed[:, tokens, : tokens * top_k].reshape(n_ep, tokens, top_k).astype(i32)
-    named = jnp.pad(named, ((0, 0), (0, height - tokens), (0, 0)), constant_values=-1)
-    named = named.reshape(1, 1, n_ep, height, top_k)
     message_rows = -(-(n_ep + tokens) // 16) * 16
-    shape = (n_ep, message_rows, n_ep, height)
-    expert = lax.broadcasted_iota(i32, shape, 0)
-    slot = lax.broadcasted_iota(i32, shape, 1)
-    block = lax.broadcasted_iota(i32, shape, 2)
-    place = lax.broadcasted_iota(i32, shape, 3)
-    hit = jnp.any(named == expert[..., None], axis=-1)
-    pick = ((slot == block) & hit) | ((block == expert) & (slot == n_ep + place) & (place < tokens))
-    pick = pick.astype(bf16).reshape(n_ep * message_rows, n_ep * height)
+    pick = call(
+        lambda *refs: pick_kernel(*refs, tokens=tokens, top_k=top_k),
+        name="pick",
+        out_shape=jax.ShapeDtypeStruct((n_ep * message_rows, n_ep * height), bf16),
+        in_specs=[in_vmem],
+        out_specs=in_vmem,
+        compiler_params=params,
+    )(near(packed))
 
     message = call(
         lambda *refs: project_kernel(*refs, tokens=tokens, n_tp=n_tp),
@@ -210,7 +254,8 @@
         out_shape=jax.ShapeDtypeStruct((n_ep, n_tp, message_rows, columns), bf16),
         in_specs=[in_vmem] * 4,
         out_specs=in_vmem,
-    )(heads_out, out_weight, packed, pick)
+        compiler_params=params,
+    )(near(heads_out), near(out_weight), near(packed), near(pick))
     message = message.reshape(n_ep * n_tp, message_rows, columns)
     message = lax.all_to_all(message, ("ep", "tp"), split_axis=0, concat_axis=0, tiled=True)
 
@@ -223,12 +268,13 @@
         ),
         in_specs=[in_vmem] * 5,
         out_specs=(in_vmem, in_vmem),
+        compiler_params=params,
     )(
-        message.reshape(n_ep, n_tp, message_rows, columns),
-        moe_gain.reshape(1, d_model),
-        gate_w,
-        up_w,
-        down_w,
+        near(message.reshape(n_ep, n_tp, message_rows, columns)),
+        near(moe_gain.reshape(1, d_model)),
+        near(gate_w.swapaxes(1, 2)),
+        near(up_w.swapaxes(1, 2)),
+        near(down_w),
     )
     lanes = part_width // size
     returned = lax.all_to_all(

time: 74.5 us -> 69.1 us (0.928)
  blocking collectives: 0 us -> 23.2 us
  starting transfers between devices: 19.3 us -> 8.59 us
  waiting for transfers between devices: 32 us -> 23.5 us
  Pallas kernels: 11.7 us -> 6.73 us
  local copies, waits for them, and re-layouts: 8.97 us -> 5.5 us
  other arithmetic: 1.69 us -> 0.81 us
    all_to_all x0 -> x2, blocking collectives: none -> 23.2 us  [the longest x1 13.8 us: fast_body(): lax.all_to_all(packed, 'ep', split_axis=0, concat_axis=0, tiled=True)]
    all_to_all x2 -> x0, waiting for transfers between devices: 11.5 us -> none  [the longest x1 6.35 us: fast_body(): parts = lax.all_to_all(parts, 'ep', split_axis=0, concat_axis=0, tiled=True)]
    all_to_all x2 -> x0, starting transfers between devices: 10.6 us -> none  [the longest x1 7.28 us: fast_body(): lax.all_to_all(packed, 'ep', split_axis=0, concat_axis=0, tiled=True)]
    all_to_all x1, waiting for transfers between devices: 7.96 us -> 10.5 us  [fast_body(): lax.all_to_all(message, ('ep', 'tp'), split_axis=0, concat_axis=0, tiled=...]
    unnamed x25 -> x30, local copies, waits for them, and re-layouts: 7.41 us -> 5.49 us
    pallas_call x1, Pallas kernels: 3.17 us -> 1.44 us  [fast_body(): call(lambda *refs: expert_kernel(*refs, tokens=tokens), name='expert', ou...]
    pallas_call x1, Pallas kernels: 1.78 us -> 0.15 us  [fast_body(): call(lambda *refs: query_kernel(*refs, tokens=tokens), name='query', out_...]
    pallas_call x1, Pallas kernels: 2.04 us -> 1.08 us  [fast_body(): call(lambda *refs: project_kernel(*refs, tokens=tokens, n_tp=n_tp), name=...]
  transfers between devices with their start and end apart: 5 -> 3, of which waited for: 5 -> 3; matrix products, arithmetic and copies ran while one was open for 7% -> 0% of each run, Pallas kernels for 0% -> 0%
where the time goes in v3:
time: 69.1 us; the launch traced here: 68.5 us
  waiting for transfers between devices  23.5 us (34%)
  blocking collectives  23.2 us (34%)
  starting transfers between devices  8.59 us (12%)
  Pallas kernels  6.73 us (10%)
  local copies, waits for them, and re-layouts  5.5 us (8%)
  other arithmetic  0.81 us (1%)
    all_to_all x1, blocking collectives, fast_body(): lax.all_to_all(packed, 'ep', split_axis=0, concat_axis=0, tiled=True)  13.8 us
    all_to_all x1, waiting for transfers between devices, fast_body(): lax.all_to_all(message, ('ep', 'tp'), split_axis=0, concat_axis=0, tiled=...  10.5 us
    all_to_all x1, blocking collectives, fast_body(): parts = lax.all_to_all(parts, 'ep', split_axis=0, concat_axis=0, tiled=True)  9.42 us
    all_to_all x1, waiting for transfers between devices, fast_body(): lax.all_to_all(down_out.reshape(n_ep * n_tp, lanes, size), ('ep', 'tp'),...  6.65 us
    all_to_all x1, waiting for transfers between devices, fast_body(): lax.all_to_all(heads_out, 'ep', split_axis=0, concat_axis=0, tiled=True)  6.32 us
    unnamed x30, local copies, waits for them, and re-layouts  5.49 us
    all_to_all x1, starting transfers between devices, fast_body(): lax.all_to_all(heads_out, 'ep', split_axis=0, concat_axis=0, tiled=True)  3.47 us
    pallas_call x1, Pallas kernels, fast_body(): call(attend_kernel, name='attend', out_shape=jax.ShapeDtypeStruct((n_ep,...  3.2 us
  transfers between devices with their start and end apart: 3, of which 3 were waited for; matrix products, arithmetic and copies ran while one was open for 0% of the time, Pallas kernels for 0%

profile of v3, /device:TPU:0, one launch (start us, length us, event | category | flops | bytes accessed | tf_op | source)
XLA Modules:
  0.0 68.5 jit_solution(1374365943308207353)
XLA Ops:
  0.0 0.0 copy-start.10
  0.0 0.0 copy-start.11
  0.0 0.7 copy-done.10
  0.7 0.0 copy-done.11
  0.7 0.0 copy-start.7
  0.7 0.7 %copy-done.7 = bf16[4,2048]{1,0:T(4,128)(2,1)S(1)} copy-done((bf16[4,2048]{1,0:T(4,128)(2,1)S(1)}, bf16[4,2048]{1,0:T(4,128)(2,1)}, u32[]{:S(2)}) %copy-start.7) | copy-done | bytes 16408
  1.4 0.6 send.1
  2.0 0.0 copy-start.9
  2.0 13.8 %all_to_all.25.refs_0_.refs_2_ = bf16[8,8,256]{2,1,0:T(8,128)(2,1)S(1)} all-to-all(bf16[8,8,256]{2,1,0:T(8,128)(2,1)S(1)} %send.1), channel_id=1, replica_groups=mesh['ep'=8,'tp'=4] {'ep'}, dimensions={0} | all-to-all | bytes 65536 | tf_op jit(solution)/shard_map/all_to_all | solution.py:214
  15.7 0.0 copy-done.9
  15.8 0.0 copy-start.5
  15.8 0.9 %copy-done.5 = bf16[256,512]{1,0:T(8,128)(2,1)S(1)} copy-done((bf16[256,512]{1,0:T(8,128)(2,1)S(1)}, bf16[256,512]{1,0:T(8,128)(2,1)}, u32[]{:S(2)}) %copy-start.5) | copy-done | bytes 262168
  16.7 0.2 query.1
  16.9 0.0 copy-start.12
  16.9 0.0 copy-start.13
  16.9 9.4 %all_to_all.26.parts_ref = f32[8,16,128]{2,1,0:T(8,128)S(1)} all-to-all(f32[8,16,128]{2,1,0:T(8,128)S(1)} %query.1), channel_id=1, replica_groups=mesh['ep'=8,'tp'=4] {'ep'}, dimensions={0} | all-to-all | bytes 131072 | tf_op jit(solution)/shard_map/all_to_all | solution.py:224
  26.3 0.0 copy-done.12
  26.3 0.0 copy-done.13
  26.3 0.0 copy-start
  26.3 1.2 %copy-done = bf16[4,1,1024,128]{3,2,1,0:T(8,128)(2,1)S(1)} copy-done((bf16[4,1,1024,128]{3,2,1,0:T(8,128)(2,1)S(1)}, bf16[4,1,1024,128]{3,2,1,0:T(8,128)(2,1)}, u32[]{:S(2)}) %copy-start) | copy-done | bytes 1048600
  27.5 0.0 copy-start.1
  27.5 1.2 %copy-done.1 = bf16[4,1,1024,128]{3,2,1,0:T(8,128)(2,1)S(1)} copy-done((bf16[4,1,1024,128]{3,2,1,0:T(8,128)(2,1)S(1)}, bf16[4,1,1024,128]{3,2,1,0:T(8,128)(2,1)}, u32[]{:S(2)}) %copy-start.1) | copy-done | bytes 1048600
  28.8 0.0 copy-start.6
  28.8 0.0 copy-start.3
  28.8 0.0 copy-start.4
  28.8 3.2 %attend.1 = bf16[8,16,128]{2,1,0:T(8,128)(2,1)} custom-call(f32[8,16,128]{2,1,0:T(8,128)S(1)} %all_to_all.26.parts_ref, bf16[4,2048]{1,0:T(4,128)(2,1)S(1)} %copy-done.7, bf16[4,1,1024,128]{3,2,1,0:T(8,128)(2,1)S(1)} %copy-done, bf16[4,1,1024,128]{3,2,1,0:T(8,128)(2,1)S(1)} %copy-done.1, s32[4]{0:T(128)S(1)} %copy-done.12, f32[16]{0:T(128)S(1)} %copy-done.13), custom_call_target="tpu_custom_call" | custom-call | tf_op jit(solution)/shard_map/attend/pallas_call | solution.py:226
  32.0 0.0 copy-start.2
  32.0 3.5 %all-to-all-start.2 = ((bf16[8,16,128]{2,1,0:T(8,128)(2,1)}), bf16[8,16,128]{2,1,0:T(8,128)(2,1)S(1)}, u32[]{:S(2)}, u32[]{:S(2)}) async-start(bf16[8,16,128]{2,1,0:T(8,128)(2,1)} %attend.1), calls=%async_computation.2 | async-start | bytes 65536 | tf_op jit(solution)/shard_map/all_to_all | solution.py:239
  35.5 0.3 pick.1.refs_3_
  35.8 6.3 %all-to-all-done.2.refs_0_ = bf16[8,16,128]{2,1,0:T(8,128)(2,1)S(1)} async-done(((bf16[8,16,128]{2,1,0:T(8,128)(2,1)}), bf16[8,16,128]{2,1,0:T(8,128)(2,1)S(1)}, u32[]{:S(2)}, u32[]{:S(2)}) %all-to-all-start.2) | async-done | bytes 32800 | tf_op jit(solution)/shard_map/all_to_all | solution.py:239
  42.1 0.0 copy-done.6
  42.1 1.1 %project.1 = bf16[8,4,16,256]{3,2,1,0:T(8,128)(2,1)} custom-call(bf16[8,16,128]{2,1,0:T(8,128)(2,1)S(1)} %all-to-all-done.2.refs_0_, bf16[512,256]{1,0:T(8,128)(2,1)S(1)} %copy-done.6, bf16[8,8,256]{2,1,0:T(8,128)(2,1)S(1)} %all_to_all.25.refs_0_.refs_2_, bf16[128,64]{1,0:T(8,128)(2,1)S(1)} %pick.1.refs_3_), custom_call_target="tpu_custom_call" | custom-call | tf_op jit(solution)/shard_map/project/pallas_call | solution.py:251
  43.2 2.6 %all-to-all-start.3 = ((bf16[32,16,256]{2,1,0:T(8,128)(2,1)}), bf16[32,16,256]{2,1,0:T(8,128)(2,1)S(1)}, u32[]{:S(2)}, u32[]{:S(2)}) async-start(bf16[32,16,256]{2,1,0:T(8,128)(2,1)} %bitcast.2), calls=%async_computation.3 | async-start | bytes 524288 | tf_op jit(solution)/shard_map/all_to_all | solution.py:260
  45.8 0.0 copy-start.8
  45.8 10.5 %all-to-all-done.3 = bf16[32,16,256]{2,1,0:T(8,128)(2,1)S(1)} async-done(((bf16[32,16,256]{2,1,0:T(8,128)(2,1)}), bf16[32,16,256]{2,1,0:T(8,128)(2,1)S(1)}, u32[]{:S(2)}, u32[]{:S(2)}) %all-to-all-start.3) | async-done | bytes 262176 | tf_op jit(solution)/shard_map/all_to_all | solution.py:260
  56.3 0.0 copy-done.3
  56.3 0.0 copy-done.4
  56.3 0.0 copy-done.2
  56.3 0.0 copy-done.8
  56.4 1.4 %expert.1 = (f32[8,16,128]{2,1,0:T(8,128)}, f32[8,2048]{1,0:T(8,128)S(1)}) custom-call(bf16[8,4,16,256]{3,2,1,0:T(8,128)(2,1)S(1)} %bitcast.15, f32[1,2048]{1,0:T(1,128)S(1)} %bitcast.18, bf16[1,192,2048]{2,1,0:T(8,128)(2,1)S(1)} %bitcast.16, bf16[1,192,2048]{2,1,0:T(8,128)(2,1)S(1)} %bitcast.17, bf16[1,192,2048]{2,1,0:T(8,128)(2,1)S(1)} %copy-done.4), custom_call_target="tpu_custom_call" | custom-call | tf_op jit(solution)/shard_map/expert/pallas_call | solution.py:262
  57.8 2.5 %all-to-all-start.4 = ((f32[32,4,128]{2,1,0:T(4,128)}), f32[32,4,128]{2,1,0:T(4,128)S(1)}, u32[]{:S(2)}, u32[]{:S(2)}) async-start(f32[32,4,128]{2,1,0:T(4,128)} %bitcast.7), calls=%async_computation.4 | async-start | bytes 131072 | tf_op jit(solution)/shard_map/all_to_all | solution.py:280
  60.4 0.0 copy-start.14
  60.4 0.6 copy-done.14
  61.0 0.1 select_reduce_fusion
  61.1 6.6 %all-to-all-done.4 = f32[32,4,128]{2,1,0:T(4,128)S(1)} async-done(((f32[32,4,128]{2,1,0:T(4,128)}), f32[32,4,128]{2,1,0:T(4,128)S(1)}, u32[]{:S(2)}, u32[]{:S(2)}) %all-to-all-start.4) | async-done | bytes 65568 | tf_op jit(solution)/shard_map/all_to_all | solution.py:280
  67.8 0.1 multiply_reduce_fusion
  67.9 0.6 fusion
  (6 shorter events, 0.0 us)
Async XLA Ops:
  0.0 0.7 copy-start.10
  0.0 0.7 copy-start.11
  0.7 0.7 %copy-start.7 = (bf16[4,2048]{1,0:T(4,128)(2,1)S(1)}, bf16[4,2048]{1,0:T(4,128)(2,1)}, u32[]{:S(2)}) copy-start(bf16[4,2048]{1,0:T(4,128)(2,1)} %hidden_ref.1) | copy-start | bytes 49156
  2.0 13.8 %copy-start.9 = (f32[2048]{0:T(1024)S(1)}, f32[2048]{0:T(1024)}, u32[]{:S(2)}) copy-start(f32[2048]{0:T(1024)} %param.16) | copy-start | bytes 24580
  15.8 1.0 %copy-start.5 = (bf16[256,512]{1,0:T(8,128)(2,1)S(1)}, bf16[256,512]{1,0:T(8,128)(2,1)}, u32[]{:S(2)}) copy-start(bf16[256,512]{1,0:T(8,128)(2,1)} %refs_2_.1) | copy-start | bytes 786436
  16.9 9.4 %copy-start.12 = (s32[4]{0:T(128)S(1)}, s32[4]{0:T(128)}, u32[]{:S(2)}) copy-start(s32[4]{0:T(128)} %lengths_ref.1) | copy-start | bytes 52
  16.9 9.4 %copy-start.13 = (f32[16]{0:T(128)S(1)}, f32[16]{0:T(128)}, u32[]{:S(2)}) copy-start(f32[16]{0:T(128)} %bias_ref.1) | copy-start | bytes 196
  26.3 1.2 %copy-start = (bf16[4,1,1024,128]{3,2,1,0:T(8,128)(2,1)S(1)}, bf16[4,1,1024,128]{3,2,1,0:T(8,128)(2,1)}, u32[]{:S(2)}) copy-start(bf16[4,1,1024,128]{3,2,1,0:T(8,128)(2,1)} %keys_ref.1) | copy-start | bytes 3145732
  27.5 1.2 %copy-start.1 = (bf16[4,1,1024,128]{3,2,1,0:T(8,128)(2,1)S(1)}, bf16[4,1,1024,128]{3,2,1,0:T(8,128)(2,1)}, u32[]{:S(2)}) copy-start(bf16[4,1,1024,128]{3,2,1,0:T(8,128)(2,1)} %values_ref.1) | copy-start | bytes 3145732
  28.8 13.3 %copy-start.6 = (bf16[512,256]{1,0:T(8,128)(2,1)S(1)}, bf16[512,256]{1,0:T(8,128)(2,1)}, u32[]{:S(2)}) copy-start(bf16[512,256]{1,0:T(8,128)(2,1)} %refs_1_.3) | copy-start | bytes 786436
  28.8 27.6 %copy-start.3 = (bf16[1,2048,192]{1,2,0:T(8,128)(2,1)S(1)}, bf16[1,2048,192]{1,2,0:T(8,128)(2,1)}, u32[]{:S(2)}) copy-start(bf16[1,2048,192]{1,2,0:T(8,128)(2,1)} %param.28) | copy-start | bytes 2359300
  28.8 27.6 %copy-start.4 = (bf16[1,192,2048]{2,1,0:T(8,128)(2,1)S(1)}, bf16[1,192,2048]{2,1,0:T(8,128)(2,1)}, u32[]{:S(2)}) copy-start(bf16[1,192,2048]{2,1,0:T(8,128)(2,1)} %refs_4_.1) | copy-start | bytes 2359300
  32.0 24.4 %copy-start.2 = (bf16[1,2048,192]{1,2,0:T(8,128)(2,1)S(1)}, bf16[1,2048,192]{1,2,0:T(8,128)(2,1)}, u32[]{:S(2)}) copy-start(bf16[1,2048,192]{1,2,0:T(8,128)(2,1)} %param.27) | copy-start | bytes 2359300
  32.0 10.1 %all-to-all-start.2 = ((bf16[8,16,128]{2,1,0:T(8,128)(2,1)}), bf16[8,16,128]{2,1,0:T(8,128)(2,1)S(1)}, u32[]{:S(2)}, u32[]{:S(2)}) async-start(bf16[8,16,128]{2,1,0:T(8,128)(2,1)} %attend.1), calls=%async_computation.2 | async-start | bytes 65536 | tf_op jit(solution)/shard_map/all_to_all | solution.py:239
  43.2 13.2 %all-to-all-start.3 = ((bf16[32,16,256]{2,1,0:T(8,128)(2,1)}), bf16[32,16,256]{2,1,0:T(8,128)(2,1)S(1)}, u32[]{:S(2)}, u32[]{:S(2)}) async-start(bf16[32,16,256]{2,1,0:T(8,128)(2,1)} %bitcast.2), calls=%async_computation.3 | async-start | bytes 524288 | tf_op jit(solution)/shard_map/all_to_all | solution.py:260
  45.8 10.6 %copy-start.8 = (f32[2048]{0:T(1024)S(1)}, f32[2048]{0:T(1024)}, u32[]{:S(2)}) copy-start(f32[2048]{0:T(1024)} %param.23) | copy-start | bytes 24580
  57.8 10.0 %all-to-all-start.4 = ((f32[32,4,128]{2,1,0:T(4,128)}), f32[32,4,128]{2,1,0:T(4,128)S(1)}, u32[]{:S(2)}, u32[]{:S(2)}) async-start(f32[32,4,128]{2,1,0:T(4,128)} %bitcast.7), calls=%async_computation.4 | async-start | bytes 131072 | tf_op jit(solution)/shard_map/all_to_all | solution.py:280
  60.4 0.7 copy-start.14

commit v4 on v3

--- a/solution.py
+++ b/solution.py
@@ -143,24 +143,31 @@
         total = total + found[:, h * tokens : (h + 1) * tokens, :]
     total = jnp.concatenate([total, jnp.zeros((n_ep, height - tokens, columns), f32)], axis=1)
     total = total.reshape(n_ep * height, columns).astype(bf16)
-    message = jnp.dot(pick_ref[...], total, preferred_element_type=f32).astype(bf16)
-    message = message.reshape(n_ep, out_ref.shape[2], columns)
+    message = jnp.dot(pick_ref[...], total, preferred_element_type=f32)
+    message = message.reshape(n_ep, pick_ref.shape[0] // n_ep, columns)
+    lanes = out_ref.shape[3]
+    starts = range(0, columns, lanes)
+    pieces = [message[:, :n_ep, c : c + lanes] for c in starts]
+    pieces += [message[:, n_ep : n_ep + tokens, c : c + lanes] for c in starts]
+    message = jnp.concatenate(pieces, axis=1).astype(bf16)
     for g in range(n_tp):
         out_ref[:, g] = message
 
 
 def expert_kernel(parts_ref, gain_ref, gate_ref, up_ref, down_ref, out_ref, own_ref, *, tokens):
-    n_ep, n_tp, height, columns = parts_ref.shape
+    n_ep, n_tp, height, _ = parts_ref.shape
     size = out_ref.shape[2]
-    pieces = []
+    count = height // (n_ep + tokens)
+    pieces, own = [], []
     for e in range(n_ep):
         piece = parts_ref[e, 0].astype(f32)
         for g in range(1, n_tp):
             piece = piece + parts_ref[e, g].astype(f32)
-        pieces.append(piece)
-    residual = jnp.concatenate(pieces, axis=1)
-    own_ref[...] = residual[n_ep:, :]
-    arrived = residual[:n_ep, :]
+        pieces += [piece[c * n_ep : (c + 1) * n_ep] for c in range(count)]
+        rest = piece[count * n_ep :]
+        own += [rest[c * tokens : (c + 1) * tokens] for c in range(count)]
+    own_ref[...] = jnp.concatenate(own, axis=1)
+    arrived = jnp.concatenate(pieces, axis=1)
     arrived = arrived * lax.rsqrt(jnp.mean(arrived * arrived, axis=-1, keepdims=True) + rms_epsilon)
     arrived = (arrived * gain_ref[...]).astype(bf16)
     across = (((1,), (1,)), ((), ()))
@@ -227,7 +234,7 @@
         attend_kernel,
         name="attend",
         out_shape=jax.ShapeDtypeStruct((n_ep, heads * tokens, size), bf16),
-        in_specs=[in_vmem] * 2 + [pl.BlockSpec(memory_space=pl.ANY)] * 2 + [in_smem] * 2,
+        in_specs=[in_vmem] * 2 + [pl.BlockSpec(memory_space=pltpu.HBM)] * 2 + [in_smem] * 2,
         out_specs=in_vmem,
         scratch_shapes=[
             pltpu.VMEM(key_cache.shape, key_cache.dtype),
@@ -248,15 +255,16 @@
         compiler_params=params,
     )(near(packed))
 
+    sent_rows = (n_ep + tokens) * columns // size
     message = call(
         lambda *refs: project_kernel(*refs, tokens=tokens, n_tp=n_tp),
         name="project",
-        out_shape=jax.ShapeDtypeStruct((n_ep, n_tp, message_rows, columns), bf16),
+        out_shape=jax.ShapeDtypeStruct((n_ep, n_tp, sent_rows, size), bf16),
         in_specs=[in_vmem] * 4,
         out_specs=in_vmem,
         compiler_params=params,
     )(near(heads_out), near(out_weight), near(packed), near(pick))
-    message = message.reshape(n_ep * n_tp, message_rows, columns)
+    message = message.reshape(n_ep * n_tp, sent_rows, size)
     message = lax.all_to_all(message, ("ep", "tp"), split_axis=0, concat_axis=0, tiled=True)
 
     down_out, own = call(
@@ -264,13 +272,13 @@
         name="expert",
         out_shape=(
             jax.ShapeDtypeStruct((n_ep, d_model // size, size), f32),
-            jax.ShapeDtypeStruct((message_rows - n_ep, d_model), f32),
+            jax.ShapeDtypeStruct((tokens, d_model), f32),
         ),
         in_specs=[in_vmem] * 5,
         out_specs=(in_vmem, in_vmem),
         compiler_params=params,
     )(
-        near(message.reshape(n_ep, n_tp, message_rows, columns)),
+        near(message.reshape(n_ep, n_tp, sent_rows, size)),
         near(moe_gain.reshape(1, d_model)),
         near(gate_w.swapaxes(1, 2)),
         near(up_w.swapaxes(1, 2)),
@@ -285,7 +293,7 @@
     matches = chosen[:, :, None] == jnp.arange(experts, dtype=i32)[None, None, :]
     mixing = jnp.sum(jnp.where(matches, route_weight[:, :, None].astype(f32), 0.0), axis=1)
     mixed = jnp.sum(mixing[:, :, None, None] * returned[None], axis=1).reshape(tokens, part_width)
-    own = lax.dynamic_slice_in_dim(own[:tokens], lax.axis_index("tp") * part_width, part_width, 1)
+    own = lax.dynamic_slice_in_dim(own, lax.axis_index("tp") * part_width, part_width, 1)
     return (own + mixed).astype(bf16)
 
 
@@ -298,6 +306,7 @@
     )
     single = gate_w.shape[0] == 1 and key_cache.shape[1] == 1
     shapes = hidden.shape[0] == 4 and key_cache.shape[3] == 128 and key_cache.shape[2] % 128 == 0
+    shapes = shapes and hidden.shape[1] // query_weight.shape[0] % 8 == 0
     return fast_body(*args) if aligned and single and shapes else plain_body(*args)
 
 

time: 69.1 us -> 67.4 us (0.975)
  waiting for transfers between devices: 23.5 us -> 21.9 us
    all_to_all x1, waiting for transfers between devices: 10.5 us -> 8.93 us  [fast_body(): lax.all_to_all(message, ('ep', 'tp'), split_axis=0, concat_axis=0, tiled=...]
where the time goes in v4:
time: 67.4 us; the launch traced here: 66.8 us
  blocking collectives  23.2 us (34%)
  waiting for transfers between devices  21.9 us (32%)
  starting transfers between devices  8.59 us (13%)
  Pallas kernels  6.71 us (10%)
  local copies, waits for them, and re-layouts  5.49 us (8%)
  other arithmetic  0.81 us (1%)
    all_to_all x1, blocking collectives, fast_body(): lax.all_to_all(packed, 'ep', split_axis=0, concat_axis=0, tiled=True)  13.8 us
    all_to_all x1, blocking collectives, fast_body(): parts = lax.all_to_all(parts, 'ep', split_axis=0, concat_axis=0, tiled=True)  9.42 us
    all_to_all x1, waiting for transfers between devices, fast_body(): lax.all_to_all(message, ('ep', 'tp'), split_axis=0, concat_axis=0, tiled=...  8.93 us
    all_to_all x1, waiting for transfers between devices, fast_body(): lax.all_to_all(down_out.reshape(n_ep * n_tp, lanes, size), ('ep', 'tp'),...  6.65 us
    all_to_all x1, waiting for transfers between devices, fast_body(): lax.all_to_all(heads_out, 'ep', split_axis=0, concat_axis=0, tiled=True)  6.32 us
    unnamed x30, local copies, waits for them, and re-layouts  5.49 us
    all_to_all x1, starting transfers between devices, fast_body(): lax.all_to_all(heads_out, 'ep', split_axis=0, concat_axis=0, tiled=True)  3.47 us
    pallas_call x1, Pallas kernels, fast_body(): call(attend_kernel, name='attend', out_shape=jax.ShapeDtypeStruct((n_ep,...  3.2 us
  transfers between devices with their start and end apart: 3, of which 3 were waited for; matrix products, arithmetic and copies ran while one was open for 0% of the time, Pallas kernels for 0%

profile of v4, /device:TPU:0, one launch (start us, length us, event | category | flops | bytes accessed | tf_op | source)
XLA Modules:
  0.0 66.8 jit_solution(13122894692325791868)
XLA Ops:
  0.0 0.0 copy-start.10
  0.0 0.0 copy-start.11
  0.0 0.7 %copy-done.10 = s32[4,2]{0,1:T(2,128)S(1)} copy-done((s32[4,2]{0,1:T(2,128)S(1)}, s32[4,2]{0,1:T(2,128)}, u32[]{:S(2)}) %copy-start.10) | copy-done | bytes 56
  0.7 0.0 copy-done.11
  0.7 0.0 copy-start.7
  0.7 0.7 %copy-done.7 = bf16[4,2048]{1,0:T(4,128)(2,1)S(1)} copy-done((bf16[4,2048]{1,0:T(4,128)(2,1)S(1)}, bf16[4,2048]{1,0:T(4,128)(2,1)}, u32[]{:S(2)}) %copy-start.7) | copy-done | bytes 16408
  1.4 0.6 send.1
  2.0 0.0 copy-start.9
  2.0 13.8 %all_to_all.25.refs_0_.refs_2_ = bf16[8,8,256]{2,1,0:T(8,128)(2,1)S(1)} all-to-all(bf16[8,8,256]{2,1,0:T(8,128)(2,1)S(1)} %send.1), channel_id=1, replica_groups=mesh['ep'=8,'tp'=4] {'ep'}, dimensions={0} | all-to-all | bytes 65536 | tf_op jit(solution)/shard_map/all_to_all | solution.py:221
  15.7 0.0 copy-done.9
  15.8 0.0 copy-start.5
  15.8 0.9 %copy-done.5 = bf16[256,512]{1,0:T(8,128)(2,1)S(1)} copy-done((bf16[256,512]{1,0:T(8,128)(2,1)S(1)}, bf16[256,512]{1,0:T(8,128)(2,1)}, u32[]{:S(2)}) %copy-start.5) | copy-done | bytes 262168
  16.7 0.2 query.1
  16.9 0.0 copy-start.12
  16.9 0.0 copy-start.13
  16.9 9.4 %all_to_all.26.parts_ref = f32[8,16,128]{2,1,0:T(8,128)S(1)} all-to-all(f32[8,16,128]{2,1,0:T(8,128)S(1)} %query.1), channel_id=1, replica_groups=mesh['ep'=8,'tp'=4] {'ep'}, dimensions={0} | all-to-all | bytes 131072 | tf_op jit(solution)/shard_map/all_to_all | solution.py:231
  26.3 0.0 copy-done.12
  26.3 0.0 copy-done.13
  26.3 0.0 copy-start
  26.3 1.2 %copy-done = bf16[4,1,1024,128]{3,2,1,0:T(8,128)(2,1)S(1)} copy-done((bf16[4,1,1024,128]{3,2,1,0:T(8,128)(2,1)S(1)}, bf16[4,1,1024,128]{3,2,1,0:T(8,128)(2,1)}, u32[]{:S(2)}) %copy-start) | copy-done | bytes 1048600
  27.5 0.0 copy-start.1
  27.5 1.2 %copy-done.1 = bf16[4,1,1024,128]{3,2,1,0:T(8,128)(2,1)S(1)} copy-done((bf16[4,1,1024,128]{3,2,1,0:T(8,128)(2,1)S(1)}, bf16[4,1,1024,128]{3,2,1,0:T(8,128)(2,1)}, u32[]{:S(2)}) %copy-start.1) | copy-done | bytes 1048600
  28.8 0.0 copy-start.6
  28.8 0.0 copy-start.3
  28.8 0.0 copy-start.4
  28.8 3.2 %attend.1 = bf16[8,16,128]{2,1,0:T(8,128)(2,1)} custom-call(f32[8,16,128]{2,1,0:T(8,128)S(1)} %all_to_all.26.parts_ref, bf16[4,2048]{1,0:T(4,128)(2,1)S(1)} %copy-done.7, bf16[4,1,1024,128]{3,2,1,0:T(8,128)(2,1)S(1)} %copy-done, bf16[4,1,1024,128]{3,2,1,0:T(8,128)(2,1)S(1)} %copy-done.1, s32[4]{0:T(128)S(1)} %copy-done.12, f32[16]{0:T(128)S(1)} %copy-done.13), custom_call_target="tpu_custom_call" | custom-call | tf_op jit(solution)/shard_map/attend/pallas_call | solution.py:233
  32.0 0.0 copy-start.2
  32.0 3.5 %all-to-all-start.2 = ((bf16[8,16,128]{2,1,0:T(8,128)(2,1)}), bf16[8,16,128]{2,1,0:T(8,128)(2,1)S(1)}, u32[]{:S(2)}, u32[]{:S(2)}) async-start(bf16[8,16,128]{2,1,0:T(8,128)(2,1)} %attend.1), calls=%async_computation.2 | async-start | bytes 65536 | tf_op jit(solution)/shard_map/all_to_all | solution.py:246
  35.5 0.3 pick.1.refs_3_
  35.8 6.3 %all-to-all-done.2.refs_0_ = bf16[8,16,128]{2,1,0:T(8,128)(2,1)S(1)} async-done(((bf16[8,16,128]{2,1,0:T(8,128)(2,1)}), bf16[8,16,128]{2,1,0:T(8,128)(2,1)S(1)}, u32[]{:S(2)}, u32[]{:S(2)}) %all-to-all-start.2) | async-done | bytes 32800 | tf_op jit(solution)/shard_map/all_to_all | solution.py:246
  42.1 0.0 copy-done.6
  42.1 1.1 %project.1 = bf16[8,4,24,128]{3,2,1,0:T(8,128)(2,1)} custom-call(bf16[8,16,128]{2,1,0:T(8,128)(2,1)S(1)} %all-to-all-done.2.refs_0_, bf16[512,256]{1,0:T(8,128)(2,1)S(1)} %copy-done.6, bf16[8,8,256]{2,1,0:T(8,128)(2,1)S(1)} %all_to_all.25.refs_0_.refs_2_, bf16[128,64]{1,0:T(8,128)(2,1)S(1)} %pick.1.refs_3_), custom_call_target="tpu_custom_call" | custom-call | tf_op jit(solution)/shard_map/project/pallas_call | solution.py:259
  43.2 2.6 %all-to-all-start.3 = ((bf16[32,24,128]{2,1,0:T(8,128)(2,1)}), bf16[32,24,128]{2,1,0:T(8,128)(2,1)S(1)}, u32[]{:S(2)}, u32[]{:S(2)}) async-start(bf16[32,24,128]{2,1,0:T(8,128)(2,1)} %bitcast.2), calls=%async_computation.3 | async-start | bytes 393216 | tf_op jit(solution)/shard_map/all_to_all | solution.py:268
  45.7 0.0 copy-start.8
  45.8 8.9 %all-to-all-done.3 = bf16[32,24,128]{2,1,0:T(8,128)(2,1)S(1)} async-done(((bf16[32,24,128]{2,1,0:T(8,128)(2,1)}), bf16[32,24,128]{2,1,0:T(8,128)(2,1)S(1)}, u32[]{:S(2)}, u32[]{:S(2)}) %all-to-all-start.3) | async-done | bytes 196640 | tf_op jit(solution)/shard_map/all_to_all | solution.py:268
  54.7 0.0 copy-done.3
  54.7 0.0 copy-done.4
  54.7 0.0 copy-done.2
  54.7 0.0 copy-done.8
  54.7 1.4 %expert.1 = (f32[8,16,128]{2,1,0:T(8,128)}, f32[4,2048]{1,0:T(4,128)S(1)}) custom-call(bf16[8,4,24,128]{3,2,1,0:T(8,128)(2,1)S(1)} %bitcast.15, f32[1,2048]{1,0:T(1,128)S(1)} %bitcast.18, bf16[1,192,2048]{2,1,0:T(8,128)(2,1)S(1)} %bitcast.16, bf16[1,192,2048]{2,1,0:T(8,128)(2,1)S(1)} %bitcast.17, bf16[1,192,2048]{2,1,0:T(8,128)(2,1)S(1)} %copy-done.4), custom_call_target="tpu_custom_call" | custom-call | tf_op jit(solution)/shard_map/expert/pallas_call | solution.py:270
  56.1 2.5 %all-to-all-start.4 = ((f32[32,4,128]{2,1,0:T(4,128)}), f32[32,4,128]{2,1,0:T(4,128)S(1)}, u32[]{:S(2)}, u32[]{:S(2)}) async-start(f32[32,4,128]{2,1,0:T(4,128)} %bitcast.7), calls=%async_computation.4 | async-start | bytes 131072 | tf_op jit(solution)/shard_map/all_to_all | solution.py:288
  58.7 0.0 copy-start.14
  58.7 0.6 copy-done.14
  59.4 0.1 select_reduce_fusion
  59.5 6.7 %all-to-all-done.4 = f32[32,4,128]{2,1,0:T(4,128)S(1)} async-done(((f32[32,4,128]{2,1,0:T(4,128)}), f32[32,4,128]{2,1,0:T(4,128)S(1)}, u32[]{:S(2)}, u32[]{:S(2)}) %all-to-all-start.4) | async-done | bytes 65568 | tf_op jit(solution)/shard_map/all_to_all | solution.py:288
  66.1 0.1 multiply_reduce_fusion
  66.2 0.6 fusion
  (5 shorter events, 0.0 us)
Async XLA Ops:
  0.0 0.7 %copy-start.10 = (s32[4,2]{0,1:T(2,128)S(1)}, s32[4,2]{0,1:T(2,128)}, u32[]{:S(2)}) copy-start(s32[4,2]{0,1:T(2,128)} %param.25) | copy-start | bytes 100
  0.0 0.7 %copy-start.11 = (s32[4]{0:T(128)S(1)}, s32[4]{0:T(128)}, u32[]{:S(2)}) copy-start(s32[4]{0:T(128)} %refs_1_.2) | copy-start | bytes 52
  0.7 0.7 %copy-start.7 = (bf16[4,2048]{1,0:T(4,128)(2,1)S(1)}, bf16[4,2048]{1,0:T(4,128)(2,1)}, u32[]{:S(2)}) copy-start(bf16[4,2048]{1,0:T(4,128)(2,1)} %hidden_ref.1) | copy-start | bytes 49156
  2.0 13.8 %copy-start.9 = (f32[2048]{0:T(1024)S(1)}, f32[2048]{0:T(1024)}, u32[]{:S(2)}) copy-start(f32[2048]{0:T(1024)} %param.16) | copy-start | bytes 24580
  15.8 1.0 %copy-start.5 = (bf16[256,512]{1,0:T(8,128)(2,1)S(1)}, bf16[256,512]{1,0:T(8,128)(2,1)}, u32[]{:S(2)}) copy-start(bf16[256,512]{1,0:T(8,128)(2,1)} %refs_2_.1) | copy-start | bytes 786436
  16.9 9.4 %copy-start.12 = (s32[4]{0:T(128)S(1)}, s32[4]{0:T(128)}, u32[]{:S(2)}) copy-start(s32[4]{0:T(128)} %lengths_ref.1) | copy-start | bytes 52
  16.9 9.4 %copy-start.13 = (f32[16]{0:T(128)S(1)}, f32[16]{0:T(128)}, u32[]{:S(2)}) copy-start(f32[16]{0:T(128)} %bias_ref.1) | copy-start | bytes 196
  26.3 1.2 %copy-start = (bf16[4,1,1024,128]{3,2,1,0:T(8,128)(2,1)S(1)}, bf16[4,1,1024,128]{3,2,1,0:T(8,128)(2,1)}, u32[]{:S(2)}) copy-start(bf16[4,1,1024,128]{3,2,1,0:T(8,128)(2,1)} %keys_ref.1) | copy-start | bytes 3145732
  27.5 1.2 %copy-start.1 = (bf16[4,1,1024,128]{3,2,1,0:T(8,128)(2,1)S(1)}, bf16[4,1,1024,128]{3,2,1,0:T(8,128)(2,1)}, u32[]{:S(2)}) copy-start(bf16[4,1,1024,128]{3,2,1,0:T(8,128)(2,1)} %values_ref.1) | copy-start | bytes 3145732
  28.8 13.3 %copy-start.6 = (bf16[512,256]{1,0:T(8,128)(2,1)S(1)}, bf16[512,256]{1,0:T(8,128)(2,1)}, u32[]{:S(2)}) copy-start(bf16[512,256]{1,0:T(8,128)(2,1)} %refs_1_.3) | copy-start | bytes 786436
  28.8 25.9 %copy-start.3 = (bf16[1,2048,192]{1,2,0:T(8,128)(2,1)S(1)}, bf16[1,2048,192]{1,2,0:T(8,128)(2,1)}, u32[]{:S(2)}) copy-start(bf16[1,2048,192]{1,2,0:T(8,128)(2,1)} %param.28) | copy-start | bytes 2359300
  28.8 25.9 %copy-start.4 = (bf16[1,192,2048]{2,1,0:T(8,128)(2,1)S(1)}, bf16[1,192,2048]{2,1,0:T(8,128)(2,1)}, u32[]{:S(2)}) copy-start(bf16[1,192,2048]{2,1,0:T(8,128)(2,1)} %refs_4_.1) | copy-start | bytes 2359300
  32.0 22.7 %copy-start.2 = (bf16[1,2048,192]{1,2,0:T(8,128)(2,1)S(1)}, bf16[1,2048,192]{1,2,0:T(8,128)(2,1)}, u32[]{:S(2)}) copy-start(bf16[1,2048,192]{1,2,0:T(8,128)(2,1)} %param.27) | copy-start | bytes 2359300
  32.0 10.1 %all-to-all-start.2 = ((bf16[8,16,128]{2,1,0:T(8,128)(2,1)}), bf16[8,16,128]{2,1,0:T(8,128)(2,1)S(1)}, u32[]{:S(2)}, u32[]{:S(2)}) async-start(bf16[8,16,128]{2,1,0:T(8,128)(2,1)} %attend.1), calls=%async_computation.2 | async-start | bytes 65536 | tf_op jit(solution)/shard_map/all_to_all | solution.py:246
  43.2 11.5 %all-to-all-start.3 = ((bf16[32,24,128]{2,1,0:T(8,128)(2,1)}), bf16[32,24,128]{2,1,0:T(8,128)(2,1)S(1)}, u32[]{:S(2)}, u32[]{:S(2)}) async-start(bf16[32,24,128]{2,1,0:T(8,128)(2,1)} %bitcast.2), calls=%async_computation.3 | async-start | bytes 393216 | tf_op jit(solution)/shard_map/all_to_all | solution.py:268
  45.7 9.0 %copy-start.8 = (f32[2048]{0:T(1024)S(1)}, f32[2048]{0:T(1024)}, u32[]{:S(2)}) copy-start(f32[2048]{0:T(1024)} %param.23) | copy-start | bytes 24580
  56.1 10.0 %all-to-all-start.4 = ((f32[32,4,128]{2,1,0:T(4,128)}), f32[32,4,128]{2,1,0:T(4,128)S(1)}, u32[]{:S(2)}, u32[]{:S(2)}) async-start(f32[32,4,128]{2,1,0:T(4,128)} %bitcast.7), calls=%async_computation.4 | async-start | bytes 131072 | tf_op jit(solution)/shard_map/all_to_all | solution.py:288
  58.7 0.7 copy-start.14
